TPU v7x, 32 devices: a whole 2x2x4 slice. The times are simulated.
32 devices in a mesh: rep: 2 (over x), fs: 4 (over z), tp: 4 (over y, core).
Axes of the slice: x: 2, y: 2, z: 4, core: 2. Of those that a mesh axis runs over, the one named last changes fastest.
Arguments:
- tokens: bfloat16 [8192, 2048], P(('rep', 'fs', 'tp')), may hold values from -6 to 6
- cotangent: bfloat16 [8192, 2048], P(('rep', 'fs', 'tp')), may hold values from -6 to 6
- gate_weight: bfloat16 [2048, 3072], P('fs', 'tp'), may hold values from -0.125 to 0.125
- up_weight: bfloat16 [2048, 3072], P('fs', 'tp'), may hold values from -0.125 to 0.125
- down_weight: bfloat16 [3072, 2048], P('tp', 'fs'), may hold values from -0.109375 to 0.109375
Outputs:
- grad_tokens: bfloat16 [8192, 2048], P(('rep', 'fs', 'tp'))
- grad_gate: float32 [2048, 3072], P('fs', 'tp')
- grad_up: float32 [2048, 3072], P('fs', 'tp')
- grad_down: float32 [3072, 2048], P('tp', 'fs')
- gate_row_norms: float32 [2048], P('fs')
- up_row_norms: float32 [2048], P('fs')
- down_row_norms: float32 [3072], P('tp')
All inputs are finite; a program needn't handle non-finite values.
Results may differ from a plain program's by a relative error of at most 0.014.
Values may be sent and summed in bfloat16 or wider, within the bound.
A program may use at most 128 MiB of HBM per device.

v0:
```python
import functools

import jax
import jax.numpy as jnp
from jax import lax
from jax.experimental import pallas as pl
from jax.experimental.pallas import tpu as pltpu
from jax.sharding import PartitionSpec as P

F32, BF16 = jnp.float32, jnp.bfloat16
MESH = pl.DeviceIdType.MESH
DOWN, GATE, UP = 0, 1, 2


def contract_last(left, right):
    return lax.dot_general(
        left, right, (((1,), (1,)), ((), ())), preferred_element_type=F32
    )


def kernel(n, tps, sliced, tok_in, cot_in, wg_in, wu_in, wd_in,
           gt_out, gg_out, gu_out, gd_out, tn_out, fn_out,
           tok, cot, wg, wu, wd, act, coef, dh, hT, gT, uT, dg, du, own, rs, xs, xr,
           pc_s, pc_r, py_r, px_r, tnorm, fnorm,
           load_sem, ag_send, ag_recv, z_send, z_recv, rs_send, rs_recv, x_send, x_recv,
           pc_ss, pc_rs, py_ss, py_rs, px_ss, px_rs, tn_ss, tn_rs, fn_ss, fn_rs):
    ny = tps // 2
    r, f, t = lax.axis_index("rep"), lax.axis_index("fs"), lax.axis_index("tp")
    y, c = lax.div(t, 2), lax.rem(t, 2)
    R, D = tok_in.shape
    T, H = tok.shape[0], wg.shape[1]
    Dn = D // n
    tcore = t + 1 - 2 * c
    core_dev, x_dev = (r, f, tcore), (1 - r, f, t)
    ty = lambda dy: lax.rem(y + dy + ny, ny) * 2 + c
    y_dev = lambda dy: (r, f, ty(dy))
    right, left = (r, lax.rem(f + 1, n), t), (r, lax.rem(f + n - 1, n), t)

    def remote(src, dst, ss, rsem, dev):
        return pltpu.make_async_remote_copy(
            src_ref=src, dst_ref=dst, send_sem=ss, recv_sem=rsem,
            device_id=dev, device_id_type=MESH)

    def arrived(dst, sem):
        remote(dst, dst, sem, sem, core_dev).wait_recv()

    def rows(start, size):
        return pl.ds(pl.multiple_of(start, size), size)

    pending = []

    half = (lambda ref: ref.at[:, rows(r * H, H)]) if sliced else (lambda ref: ref)
    half_d = (lambda ref: ref.at[rows(r * H, H)]) if sliced else (lambda ref: ref)
    my_rows = rows((r * tps + t) * R, R)
    loads = [
        pltpu.make_async_copy(src, dst, load_sem.at[i]) for i, (src, dst) in enumerate([
            (tok_in, tok.at[my_rows]),
            (half(wg_in), wg.at[rows(f * Dn, Dn)]),
            (half(wu_in), wu.at[rows(f * Dn, Dn)]),
            (cot_in, cot.at[my_rows]),
            (half_d(wd_in), wd.at[:, rows(f * Dn, Dn)]),
        ])]
    for load in loads:
        load.start()

    barrier = pltpu.get_barrier_semaphore()
    for i in range(1, tps):
        pl.semaphore_signal(barrier, inc=1, device_id=(r, f, lax.rem(t + i, tps)), device_id_type=MESH)
    for i in range(1, n):
        pl.semaphore_signal(barrier, inc=1, device_id=(r, lax.rem(f + i, n), t), device_id_type=MESH)
    pl.semaphore_signal(barrier, inc=1, device_id=x_dev, device_id_type=MESH)
    pl.semaphore_wait(barrier, tps - 1 + n - 1 + 1)

    counts = [0, 0]
    bufs = (tok, cot)

    def part(a, slot, piece):
        if piece is None:
            return bufs[a].at[rows(slot * R, R)]
        return bufs[a].at[rows(slot * R + piece * (R // 2), R // 2)]

    def send_block(a, slot, piece, dev):
        view = part(a, slot, piece)
        copy = remote(view, view, ag_send.at[a, counts[a]], ag_recv.at[a, slot, piece or 0], dev)
        counts[a] += 1
        copy.start()
        pending.append(copy)

    def block_arrived(a, slot, piece):
        arrived(part(a, slot, piece), ag_recv.at[a, slot, piece or 0])

    slot_of = lambda rr, tt: rr * tps + tt

    def own_out(a):
        send_block(a, slot_of(r, t), None, x_dev)
        for dy in range(1, ny):
            send_block(a, slot_of(r, t), None, y_dev(dy))

    def own_core(a):
        send_block(a, slot_of(r, t), None, core_dev)

    def first_arrivals(a):
        slot = slot_of(1 - r, t)
        block_arrived(a, slot, None)
        for dy in range(1, ny):
            send_block(a, slot, 1, y_dev(dy))
        sent = [slot]
        for dy in range(1, ny):
            slot = slot_of(r, ty(-dy))
            block_arrived(a, slot, None)
            send_block(a, slot, 0, x_dev)
            sent.append(slot)
        return sent

    def to_core(a, slots):
        for slot in slots:
            send_block(a, slot, None, core_dev)

    def diagonal(a):
        for dy in range(1, ny):
            slot = slot_of(1 - r, ty(-dy))
            for piece in (0, 1):
                block_arrived(a, slot, piece)
                send_block(a, slot, piece, core_dev)

    def from_core(a):
        block_arrived(a, slot_of(r, tcore), None)
        block_arrived(a, slot_of(1 - r, tcore), None)
        for dy in range(1, ny):
            other = ty(dy) + 1 - 2 * c
            block_arrived(a, slot_of(r, other), None)
            for piece in (0, 1):
                block_arrived(a, slot_of(1 - r, other), piece)

    def weight(w, k):
        if w == DOWN:
            return wd.at[:, rows(k * Dn, Dn)]
        return (wg if w == GATE else wu).at[rows(k * Dn, Dn)]

    def weights_step(ws, s):
        for way, to, origin, has, sends in (
            (0, right, f - s, f - s >= 0, f + 1 < n),
            (1, left, f + s, f + s < n, f > 0),
        ):
            @pl.when(has)
            def _():
                for w in ws:
                    if s:
                        arrived(weight(w, origin), z_recv.at[w, origin])
                if s < n - 1:
                    @pl.when(sends)
                    def _():
                        for w in ws:
                            view = weight(w, origin)
                            remote(view, view, z_send.at[w, way, s], z_recv.at[w, origin], to).start()

    def weights_sent(ws):
        for s in range(n - 1):
            for way, to, origin, has, sends in (
                (0, right, f - s, f - s >= 0, f + 1 < n),
                (1, left, f + s, f + s < n, f > 0),
            ):
                @pl.when(jnp.logical_and(has, sends))
                def _():
                    for w in ws:
                        view = weight(w, origin)
                        remote(view, view, z_send.at[w, way, s], z_recv.at[w, origin], to).wait_send()

    for load in loads[:3]:
        load.wait()
    own_out(0)
    own_core(0)
    weights_step((GATE, UP), 0)
    for load in loads[3:]:
        load.wait()
    own_core(1)
    for s in range(1, n - 2):
        weights_step((GATE, UP), s)
    got = first_arrivals(0)
    own_out(1)
    to_core(0, got)
    for s in range(max(1, n - 2), n - 1):
        weights_step((GATE, UP), s)
    weights_step((DOWN,), 0)
    diagonal(0)
    from_core(0)
    weights_step((GATE, UP), n - 1)

    MB = min(512, T)
    EB = 128

    @pl.loop(0, T // MB)
    def _(i):
        blk = rows(i * MB, MB)
        act[blk] = jnp.dot(tok[blk], wg[...], preferred_element_type=F32)
        coef[blk] = jnp.dot(tok[blk], wu[...], preferred_element_type=F32)

    @pl.loop(0, T // EB)
    def _(i):
        blk = rows(i * EB, EB)
        gate, up = act[blk], coef[blk]
        sig = jax.nn.sigmoid(gate)
        a = gate * sig
        act[blk] = a
        coef[blk] = up * sig * (1.0 + gate * (1.0 - sig))
        hT[:, blk] = (a * up).astype(BF16).T

    got = first_arrivals(1)
    to_core(1, got)
    for s in range(1, n - 1):
        weights_step((DOWN,), s)
    diagonal(1)
    from_core(1)

    sources = {DOWN: (hT, cot), GATE: (gT, tok), UP: (uT, tok)}

    def own_part(w, d):
        lhs, rhs = sources[w]
        own[...] = jnp.dot(lhs[...], rhs[:, rows(d * Dn, Dn)], preferred_element_type=F32)

    def grads_out(w):
        @pl.loop(0, n - 1)
        def _(i):
            dist = n - 1 - i
            for to, d, has, more in (
                (right, f + dist, f + dist < n, f > 0),
                (left, f - dist, f - dist >= 0, f < n - 1),
            ):
                @pl.when(has)
                def _():
                    own_part(w, d)

                    @pl.when(more)
                    def _():
                        arrived(rs.at[w, d], rs_recv.at[w, d])
                        rs[w, d] = (own[...] + rs[w, d].astype(F32)).astype(BF16)

                    @pl.when(jnp.logical_not(more))
                    def _():
                        rs[w, d] = own[...].astype(BF16)

                    there = d if to is right else jnp.where(d == f - 1, n, d)
                    remote(rs.at[w, d], rs.at[w, there], rs_send.at[w, d], rs_recv.at[w, there], to).start()

    def grads_sent(w):
        @pl.loop(0, n)
        def _(d):
            @pl.when(d != f)
            def _():
                remote(rs.at[w, d], rs.at[w, d], rs_send.at[w, d], rs_recv.at[w, d], right).wait_send()

    def grads_final(w):
        own_part(w, f)

        @pl.when(f > 0)
        def _():
            arrived(rs.at[w, f], rs_recv.at[w, f])
            own[...] += rs[w, f].astype(F32)

        @pl.when(f < n - 1)
        def _():
            arrived(rs.at[w, n], rs_recv.at[w, n])
            own[...] += rs[w, n].astype(F32)

        xs[w] = own[...].astype(BF16)
        remote(xs.at[w], xr.at[w], x_send.at[w], x_recv.at[w], x_dev).start()

    grads_out(DOWN)
    weights_step((DOWN,), n - 1)

    @pl.loop(0, T // MB)
    def _(i):
        blk = rows(i * MB, MB)
        dh[blk] = contract_last(cot[blk], wd[...])

    @pl.loop(0, T // EB)
    def _(i):
        blk = rows(i * EB, EB)
        dhid = dh[blk]
        a = (dhid * coef[blk]).astype(BF16)
        b = (dhid * act[blk]).astype(BF16)
        dg[blk] = a
        du[blk] = b
        gT[:, blk] = a.T
        uT[:, blk] = b.T

    KB = min(512, D)

    def partial(slot, finish):
        blk = rows(slot * R, R)

        @pl.loop(0, D // KB)
        def _(k):
            cols = rows(k * KB, KB)
            finish(cols, contract_last(dg[blk], wg[cols]) + contract_last(du[blk], wu[cols]))

    for i in range(2 * ny):
        def put(cols, value):
            pc_s[i, :, cols] = value.astype(BF16)
        partial(slot_of(i // ny, (i % ny) * 2 + 1 - c), put)
        copy = remote(pc_s.at[i], pc_r.at[i], pc_ss.at[i], pc_rs.at[i], core_dev)
        copy.start()
        pending.append(copy)
    grads_out(GATE)

    for part_r in (1 - r, r):
        for dy in list(range(1, ny)) + [0]:
            yy = lax.rem(y + dy, ny)
            i = part_r * ny + yy
            arrived(pc_r.at[i], pc_rs.at[i])

            def put(cols, value):
                pc_r[i, :, cols] = (value + pc_r[i, :, cols].astype(F32)).astype(BF16)
            partial(slot_of(part_r, yy * 2 + c), put)
            if dy:
                copy = remote(pc_r.at[i], py_r.at[dy - 1, part_r], py_ss.at[dy - 1, part_r],
                              py_rs.at[dy - 1, part_r], y_dev(dy))
                copy.start()
                pending.append(copy)
    grads_out(UP)
    grads_final(DOWN)

    def add_y(part_r):
        i = part_r * ny + y
        for dy in range(1, ny):
            arrived(py_r.at[dy - 1, part_r], py_rs.at[dy - 1, part_r])

    add_y(1 - r)
    iother = (1 - r) * ny + y
    EC = 64

    @pl.loop(0, R // EC)
    def _(k):
        blk = rows(k * EC, EC)
        total = pc_r[iother, blk].astype(F32)
        for dy in range(1, ny):
            total += py_r[dy - 1, 1 - r, blk].astype(F32)
        pc_r[iother, blk] = total.astype(BF16)

    copy = remote(pc_r.at[iother], px_r, px_ss, px_rs, x_dev)
    copy.start()
    pending.append(copy)
    grads_final(GATE)
    grads_final(UP)

    def squares(value):
        return jnp.sum(value * value, axis=0, keepdims=True)

    tnorm[t] = jnp.zeros(tnorm.shape[1:], F32)
    fnorm[f] = jnp.zeros(fnorm.shape[1:], F32)

    def finish(w, buf, out, at):
        value = buf.astype(F32)
        turned = value.T
        if w == DOWN:
            out[at] = buf
            return squares(turned)
        out[at] = turned.astype(BF16)
        return squares(value)

    def exchange_norms(table, me, count, ss, rsem, dev):
        for i in range(1, count):
            copy = remote(table.at[me], table.at[me], ss.at[i - 1], rsem.at[me], dev(i))
            copy.start()
            pending.append(copy)

    arrived(xr.at[DOWN], x_recv.at[DOWN])
    fnorm[f, pl.ds(r, 1)] = finish(DOWN, xs[DOWN], gd_out, r)
    fnorm[f, pl.ds(1 - r, 1)] = finish(DOWN, xr[DOWN], gd_out, 1 - r)
    exchange_norms(fnorm, f, n, fn_ss, fn_rs, lambda i: (r, lax.rem(f + i, n), t))
    for row, (w, out) in enumerate(((GATE, gg_out), (UP, gu_out))):
        arrived(xr.at[w], x_recv.at[w])
        mine = finish(w, xs[w], out, r)
        theirs = finish(w, xr[w], out, 1 - r)
        tnorm[t, pl.ds(row, 1)] = mine + theirs
    exchange_norms(tnorm, t, tps, tn_ss, tn_rs, lambda i: (r, f, lax.rem(t + i, tps)))

    add_y(r)
    arrived(px_r, px_rs)
    imine = r * ny + y

    @pl.loop(0, R // EC)
    def _(k):
        blk = rows(k * EC, EC)
        total = pc_r[imine, blk].astype(F32) + px_r[blk].astype(F32)
        for dy in range(1, ny):
            total += py_r[dy - 1, r, blk].astype(F32)
        gt_out[blk] = total.astype(BF16)

    for i in range(1, n):
        k = lax.rem(f + i, n)
        arrived(fnorm.at[k], fn_rs.at[k])
    fn_out[...] = jnp.sum(fnorm[...], axis=0)
    for i in range(1, tps):
        k = lax.rem(t + i, tps)
        arrived(tnorm.at[k], tn_rs.at[k])
    tn_out[...] = jnp.sum(tnorm[...], axis=0)

    for copy in pending:
        copy.wait_send()
    weights_sent((GATE, UP, DOWN))
    for w in (DOWN, GATE, UP):
        grads_sent(w)
        remote(xs.at[w], xr.at[w], x_send.at[w], x_recv.at[w], x_dev).wait_send()


def local(tokens, cotangent, gate_weight, up_weight, down_weight):
    n, tps = lax.axis_size("fs"), lax.axis_size("tp")
    ny = tps // 2
    R, D = tokens.shape
    H = gate_weight.shape[1] // 2
    T, Dn = 2 * tps * R, D // n
    sliced = H % 128 == 0
    if not sliced:
        r = lax.axis_index("rep")
        gate_weight = lax.dynamic_slice_in_dim(gate_weight, r * H, H, 1)
        up_weight = lax.dynamic_slice_in_dim(up_weight, r * H, H, 1)
        down_weight = lax.dynamic_slice_in_dim(down_weight, r * H, H, 0)
    blocks = 2 * tps
    vmem = pltpu.VMEM
    dma = lambda *shape: pltpu.SemaphoreType.DMA(shape)
    shape = jax.ShapeDtypeStruct
    any_spec, vmem_spec = pl.BlockSpec(memory_space=pl.ANY), pl.BlockSpec(memory_space=vmem)
    flops = 2 * 8 * T * D * H
    gt, gg, gu, gd, tn, fn = pl.pallas_call(
        functools.partial(kernel, n, tps, sliced),
        out_shape=(
            shape((R, D), BF16), shape((2, Dn, H), BF16), shape((2, Dn, H), BF16),
            shape((2, H, Dn), BF16), shape((8, Dn), F32), shape((8, H), F32)),
        in_specs=[any_spec] * 5,
        out_specs=(vmem_spec,) * 6,
        scratch_shapes=[
            vmem((T, D), BF16), vmem((T, D), BF16),
            vmem((D, H), BF16), vmem((D, H), BF16), vmem((H, D), BF16),
            vmem((T, H), F32), vmem((T, H), F32), vmem((T, H), F32),
            vmem((H, T), BF16), vmem((H, T), BF16), vmem((H, T), BF16),
            vmem((T, H), BF16), vmem((T, H), BF16), vmem((H, Dn), F32),
            vmem((3, n + 1, H, Dn), BF16), vmem((3, H, Dn), BF16), vmem((3, H, Dn), BF16),
            vmem((2 * ny, R, D), BF16), vmem((2 * ny, R, D), BF16),
            vmem((max(ny - 1, 1), 2, R, D), BF16), vmem((R, D), BF16),
            vmem((tps, 8, Dn), F32), vmem((n, 8, H), F32),
            dma(5), dma(2, 4 * blocks), dma(2, blocks, 2), dma(3, 2, n), dma(3, n),
            dma(3, n), dma(3, n + 1), dma(3), dma(3),
            dma(2 * ny), dma(2 * ny), dma(max(ny - 1, 1), 2), dma(max(ny - 1, 1), 2),
            pltpu.SemaphoreType.DMA, pltpu.SemaphoreType.DMA, dma(tps), dma(tps), dma(n), dma(n),
        ],
        compiler_params=pltpu.CompilerParams(
            collective_id=0, has_side_effects=True, vmem_limit_bytes=67043328),
        cost_estimate=pl.CostEstimate(flops=flops, bytes_accessed=16 << 20, transcendentals=T * H),
    )(tokens, cotangent, gate_weight, up_weight, down_weight)
    wide = lambda part: jnp.concatenate([part[0], part[1]], axis=1).astype(F32)
    return (
        gt,
        wide(gg),
        wide(gu),
        gd.reshape(2 * H, Dn).astype(F32),
        tn[0],
        tn[1],
        jnp.concatenate([fn[0], fn[1]]),
    )


def solution(mesh):
    placed = (
        P(("rep", "fs", "tp"), None),
        P(("rep", "fs", "tp"), None),
        P("fs", "tp"),
        P("fs", "tp"),
        P("tp", "fs"),
    )
    return jax.shard_map(
        local,
        mesh=mesh,
        in_specs=placed,
        out_specs=(
            P(("rep", "fs", "tp"), None),
            P("fs", "tp"),
            P("fs", "tp"),
            P("tp", "fs"),
            P("fs"),
            P("fs"),
            P("tp"),
        ),
        check_vma=False,
    )
```

profile of v0, /device:TPU:17, one launch (start us, length us, event | category | flops | bytes accessed | tf_op | source)
XLA Modules:
  0.0 219.3 jit_solution(3656239378229833533)
XLA Ops:
  0.6 209.2 %shard_map.108 = (bf16[256,2048]{1,0:T(8,128)(2,1)}, bf16[2,512,384]{2,1,0:T(8,128)(2,1)}, bf16[2,512,384]{2,1,0:T(8,128)(2,1)}, bf16[2,384,512]{2,1,0:T(8,128)(...) custom-call(bf16[256,2048]{1,0:T(8,128)(2,1)} %tok_in.1, bf16[256,2048]{1,0:T(8,128)(2,1)} %cot_in.1, bf16[512,768]{1,0:T(8,128)(2,1)} %wg_in.1, ...), custom_call_target="tpu_custom_call" | custom-call | flops 25769803776 | bytes 16777216 | tf_op jit(solution)/shard_map/pallas_call | solution.py:425
  209.8 0.0 copy-start.1
  209.8 0.0 copy-start.2
  209.9 1.4 fusion
  211.3 0.8 slice_reduce_fusion.1
  212.1 0.6 pad_maximum_fusion
  212.7 2.5 %bitcast_convert_fusion = f32[768,512]{1,0:T(8,128)} fusion(bf16[2,384,512]{2,1,0:T(8,128)(2,1)} %get-tuple-element.16), kind=kLoop, calls=%fused_computation.2 | loop fusion | flops 393216 | bytes 2359296 | tf_op jit(solution)/shard_map/convert_element_type | solution.py:456
  215.2 0.0 copy-done.1
  215.2 0.0 copy-done.2
  215.2 0.2 slice_bitcast_fusion.1
  215.4 1.2 maximum_convert_fusion.1
  216.6 0.0 copy-start
  216.6 1.2 maximum_convert_fusion
  217.9 0.4 copy-done
  218.3 1.0 copy.13
Async XLA Ops:
  209.8 5.4 %copy-start.1 = (bf16[2,512,384]{2,1,0:T(8,128)(2,1)S(1)}, bf16[2,512,384]{2,1,0:T(8,128)(2,1)}, u32[]{:S(2)}) copy-start(bf16[2,512,384]{2,1,0:T(8,128)(2,1)} %get-tuple-element.14) | copy-start | bytes 2359300
  209.8 5.3 %copy-start.2 = (bf16[2,512,384]{2,1,0:T(8,128)(2,1)S(1)}, bf16[2,512,384]{2,1,0:T(8,128)(2,1)}, u32[]{:S(2)}) copy-start(bf16[2,512,384]{2,1,0:T(8,128)(2,1)} %get-tuple-element.15) | copy-start | bytes 2359300
  216.6 1.7 copy-start
where the time goes:
time: 220 us; the launch traced here: 219 us
  Pallas kernels  209 us (95%)
  other arithmetic  5.59 us (3%)
  local copies, waits for them, and re-layouts  3.82 us (2%)
    pallas_call x1, Pallas kernels, local(): pl.pallas_call(functools.partial(kernel, n, tps, sliced), out_shape=(shap...  209 us

commit v1 on v0

v1 whole, which is shorter than its diff:
```python
import functools

import jax
import jax.numpy as jnp
from jax import lax
from jax.experimental import pallas as pl
from jax.experimental.pallas import tpu as pltpu
from jax.sharding import PartitionSpec as P

F32, BF16 = jnp.float32, jnp.bfloat16
MESH = pl.DeviceIdType.MESH
DOWN, GATE, UP = 0, 1, 2


def contract_last(left, right):
    return lax.dot_general(
        left, right, (((1,), (1,)), ((), ())), preferred_element_type=F32
    )


def kernel(n, tps, sliced, groups, tok_in, cot_in, wg_in, wu_in, wd_in,
           gt_out, gg_out, gu_out, gd_out, tn_out, fn_out,
           tok, cot, wg, wu, wd, act, coef, dh, hT, gT, uT, dg, du, own, rs, xs, xr,
           pc_s, pc_r, hx_r, hy_r, py_r, px_r, tnorm, fnorm,
           load_sem, ag_send, tok_recv, cot_recv, z_send, z_recv, rs_send, rs_recv,
           x_send, x_recv, pc_ss, pc_rs, hx_ss, hx_rs, hy_ss, hy_rs, py_ss, py_rs,
           px_ss, px_rs, tn_ss, tn_rs, fn_ss, fn_rs):
    ny = tps // 2
    r, f, t = lax.axis_index("rep"), lax.axis_index("fs"), lax.axis_index("tp")
    y, c = lax.div(t, 2), lax.rem(t, 2)
    R, D = tok_in.shape
    T, H = tok.shape[0], wg.shape[1]
    Dn, half_rows, chunk = D // n, R // 2, D // groups
    tcore = t + 1 - 2 * c
    core_dev, x_dev = (r, f, tcore), (1 - r, f, t)
    yat = lambda dy: lax.rem(y + dy + ny, ny)
    ty = lambda dy: yat(dy) * 2 + c
    y_dev = lambda dy: (r, f, ty(dy))
    right, left = (r, lax.rem(f + 1, n), t), (r, lax.rem(f + n - 1, n), t)
    others = range(1, ny)

    def remote(src, dst, ss, rsem, dev):
        return pltpu.make_async_remote_copy(
            src_ref=src, dst_ref=dst, send_sem=ss, recv_sem=rsem,
            device_id=dev, device_id_type=MESH)

    def arrived(dst, sem):
        remote(dst, dst, sem, sem, core_dev).wait_recv()

    def rows(start, size):
        return pl.ds(pl.multiple_of(start, size), size)

    pending = []

    def send(*args):
        copy = remote(*args)
        copy.start()
        pending.append(copy)

    half = (lambda ref: ref.at[:, rows(r * H, H)]) if sliced else (lambda ref: ref)
    half_d = (lambda ref: ref.at[rows(r * H, H)]) if sliced else (lambda ref: ref)
    my_rows = rows((r * tps + t) * R, R)
    loads = [
        pltpu.make_async_copy(src, dst, load_sem.at[i]) for i, (src, dst) in enumerate([
            (tok_in, tok.at[my_rows]),
            (half(wg_in), wg.at[rows(f * Dn, Dn)]),
            (half(wu_in), wu.at[rows(f * Dn, Dn)]),
            (cot_in, cot.at[my_rows]),
            (half_d(wd_in), wd.at[:, rows(f * Dn, Dn)]),
        ])]
    for load in loads:
        load.start()

    barrier = pltpu.get_barrier_semaphore()
    for i in range(1, tps):
        pl.semaphore_signal(barrier, inc=1, device_id=(r, f, lax.rem(t + i, tps)), device_id_type=MESH)
    for i in range(1, n):
        pl.semaphore_signal(barrier, inc=1, device_id=(r, lax.rem(f + i, n), t), device_id_type=MESH)
    pl.semaphore_signal(barrier, inc=1, device_id=x_dev, device_id_type=MESH)
    pl.semaphore_wait(barrier, tps - 1 + n - 1 + 1)

    sent = [0]

    def send_piece(view, sem, dev):
        send(view, view, ag_send.at[sent[0]], sem, dev)
        sent[0] += 1

    slot_of = lambda rr, tt: rr * tps + tt

    def tok_piece(slot, h):
        return tok.at[rows(slot * R + h * half_rows, half_rows)], tok_recv.at[slot, h]

    def cot_piece(slot, g, h):
        at = rows(slot * R, R) if h is None else rows(slot * R + h * half_rows, half_rows)
        return cot.at[at, rows(g * chunk, chunk)], cot_recv.at[slot, g, h or 0]

    mine, beside = slot_of(r, t), slot_of(1 - r, t)
    along = lambda dy: slot_of(r, ty(-dy))
    diagonal = lambda dy: slot_of(1 - r, ty(-dy))
    cored = lambda tt: tt + 1 - 2 * c

    def tok_out(to_x, to_y):
        send_piece(*tok_piece(mine, to_x), x_dev)
        for dy in others:
            send_piece(*tok_piece(mine, to_y), y_dev(dy))

    def tok_first():
        arrived(*tok_piece(beside, 1))
        for dy in others:
            send_piece(*tok_piece(beside, 1), y_dev(dy))
        for dy in others:
            arrived(*tok_piece(along(dy), 0))
            send_piece(*tok_piece(along(dy), 0), x_dev)

    def tok_first_core():
        send_piece(*tok_piece(beside, 1), core_dev)
        for dy in others:
            send_piece(*tok_piece(along(dy), 0), core_dev)

    def tok_second():
        for slot, h in [(beside, 0)] + [(along(dy), 1) for dy in others]:
            arrived(*tok_piece(slot, h))
            send_piece(*tok_piece(slot, h), core_dev)

    def tok_diagonal():
        for dy in others:
            for h in (0, 1):
                arrived(*tok_piece(diagonal(dy), h))
                send_piece(*tok_piece(diagonal(dy), h), core_dev)

    def tok_from_core():
        for dy in range(ny):
            for rr in (r, 1 - r):
                for h in (0, 1):
                    arrived(*tok_piece(slot_of(rr, cored(ty(dy))), h))

    def cot_out(g):
        send_piece(*cot_piece(mine, g, None), x_dev)
        for dy in others:
            send_piece(*cot_piece(mine, g, None), y_dev(dy))

    def cot_first(g):
        arrived(*cot_piece(beside, g, None))
        for dy in others:
            send_piece(*cot_piece(beside, g, 1), y_dev(dy))
        for dy in others:
            arrived(*cot_piece(along(dy), g, None))
            send_piece(*cot_piece(along(dy), g, 0), x_dev)

    def cot_first_core(g):
        for slot in [beside] + [along(dy) for dy in others]:
            send_piece(*cot_piece(slot, g, None), core_dev)

    def cot_diagonal(g):
        for dy in others:
            for h in (0, 1):
                arrived(*cot_piece(diagonal(dy), g, h))
                send_piece(*cot_piece(diagonal(dy), g, h), core_dev)

    def cot_from_core(g):
        arrived(*cot_piece(slot_of(r, tcore), g, None))
        arrived(*cot_piece(slot_of(1 - r, tcore), g, None))
        for dy in others:
            arrived(*cot_piece(slot_of(r, cored(ty(dy))), g, None))
            for h in (0, 1):
                arrived(*cot_piece(slot_of(1 - r, cored(ty(dy))), g, h))

    def weight(w, k):
        if w == DOWN:
            return wd.at[:, rows(k * Dn, Dn)]
        return (wg if w == GATE else wu).at[rows(k * Dn, Dn)]

    def ways(s):
        return ((0, right, f - s, f - s >= 0, f + 1 < n), (1, left, f + s, f + s < n, f > 0))

    def weights_step(w, s):
        for way, to, origin, has, sends in ways(s):
            @pl.when(has)
            def _():
                view = weight(w, origin)
                if s:
                    arrived(view, z_recv.at[w, origin])
                if s < n - 1:
                    @pl.when(sends)
                    def _():
                        remote(view, view, z_send.at[w, way, s], z_recv.at[w, origin], to).start()

    def weights_sent(w):
        for s in range(n - 1):
            for way, to, origin, has, sends in ways(s):
                @pl.when(jnp.logical_and(has, sends))
                def _():
                    view = weight(w, origin)
                    remote(view, view, z_send.at[w, way, s], z_recv.at[w, origin], to).wait_send()

    MB = min(512, T)
    EB = 128
    most = (n - 1) * Dn
    most_at = jnp.where(f == n - 1, Dn, 0)
    last_at = jnp.where(f == n - 1, 0, most)

    def gate_up_most(lo, hi):
        @pl.loop(lo, hi)
        def _(i):
            blk, cols = rows(i * MB, MB), pl.ds(pl.multiple_of(most_at, Dn), most)
            act[blk] = jnp.dot(tok[blk, cols], wg[cols], preferred_element_type=F32)
            coef[blk] = jnp.dot(tok[blk, cols], wu[cols], preferred_element_type=F32)

    def gate_up_last():
        @pl.loop(0, T // MB)
        def _(i):
            blk, cols = rows(i * MB, MB), rows(last_at, Dn)
            act[blk] += jnp.dot(tok[blk, cols], wg[cols], preferred_element_type=F32)
            coef[blk] += jnp.dot(tok[blk, cols], wu[cols], preferred_element_type=F32)

        @pl.loop(0, T // EB)
        def _(i):
            blk = rows(i * EB, EB)
            gate, up = act[blk], coef[blk]
            sig = jax.nn.sigmoid(gate)
            a = gate * sig
            act[blk] = a
            coef[blk] = up * sig * (1.0 + gate * (1.0 - sig))
            hT[:, blk] = (a * up).astype(BF16).T

    def hidden_grads():
        @pl.loop(0, T // MB)
        def _(i):
            blk = rows(i * MB, MB)
            dh[blk] = contract_last(cot[blk], wd[...])

        @pl.loop(0, T // EB)
        def _(i):
            blk = rows(i * EB, EB)
            dhid = dh[blk]
            a = (dhid * coef[blk]).astype(BF16)
            b = (dhid * act[blk]).astype(BF16)
            dg[blk] = a
            du[blk] = b
            gT[:, blk] = a.T
            uT[:, blk] = b.T

    sources = {DOWN: (hT, cot), GATE: (gT, tok), UP: (uT, tok)}

    def own_part(w, d):
        lhs, rhs = sources[w]
        own[...] = jnp.dot(lhs[...], rhs[:, rows(d * Dn, Dn)], preferred_element_type=F32)

    def grad_edge(w, d):
        @pl.when(jnp.where(f == 0, d > 0, jnp.logical_and(f == n - 1, d < n - 1)))
        def _():
            own_part(w, d)
            rs[w, d] = own[...].astype(BF16)
            there = jnp.where(jnp.logical_and(f > 0, d == f - 1), n, d)
            to = (r, jnp.where(f == 0, 1, n - 2), t)
            remote(rs.at[w, d], rs.at[w, there], rs_send.at[w, d], rs_recv.at[w, there], to).start()

    def grad_edge_group(w, g):
        per = n // groups

        @pl.loop(0, per)
        def _(i):
            grad_edge(w, g * per + i)

    def grad_edge_all(w):
        @pl.loop(0, n - 1)
        def _(i):
            grad_edge(w, jnp.where(f == 0, n - 1 - i, i))

    def grad_through(w, first, last):
        @pl.loop(0, first - last + 1)
        def _(i):
            dist = first - i
            for to, d, has in (
                (right, f + dist, jnp.logical_and(f + dist < n, f > 0)),
                (left, f - dist, jnp.logical_and(f - dist >= 0, f < n - 1)),
            ):
                @pl.when(has)
                def _():
                    own_part(w, d)
                    arrived(rs.at[w, d], rs_recv.at[w, d])
                    rs[w, d] = (own[...] + rs[w, d].astype(F32)).astype(BF16)
                    there = d if to is right else jnp.where(d == f - 1, n, d)
                    remote(rs.at[w, d], rs.at[w, there], rs_send.at[w, d], rs_recv.at[w, there], to).start()

    def grads_sent(w):
        @pl.loop(0, n)
        def _(d):
            @pl.when(d != f)
            def _():
                remote(rs.at[w, d], rs.at[w, d], rs_send.at[w, d], rs_recv.at[w, d], right).wait_send()

    def grad_final(w):
        own_part(w, f)

        @pl.when(f > 0)
        def _():
            arrived(rs.at[w, f], rs_recv.at[w, f])
            own[...] += rs[w, f].astype(F32)

        @pl.when(f < n - 1)
        def _():
            arrived(rs.at[w, n], rs_recv.at[w, n])
            own[...] += rs[w, n].astype(F32)

        xs[w] = own[...].astype(BF16)
        remote(xs.at[w], xr.at[w], x_send.at[w], x_recv.at[w], x_dev).start()

    KB = min(512, D)

    def partial(slot, finish):
        blk = rows(slot * R, R)

        @pl.loop(0, D // KB)
        def _(k):
            cols = rows(k * KB, KB)
            finish(cols, contract_last(dg[blk], wg[cols]) + contract_last(du[blk], wu[cols]))

    at_of = lambda rr, yy: rr * ny + yy

    def partial_for_core(rr, dy):
        i = at_of(rr, yat(dy))

        def put(cols, value):
            pc_s[i, :, cols] = value.astype(BF16)
        partial(slot_of(rr, cored(ty(dy))), put)
        send(pc_s.at[i], pc_r.at[i], pc_ss.at[i], pc_rs.at[i], core_dev)

    def partial_own(rr, dy):
        i = at_of(rr, yat(dy))
        arrived(pc_r.at[i], pc_rs.at[i])

        def put(cols, value):
            pc_r[i, :, cols] = (value + pc_r[i, :, cols].astype(F32)).astype(BF16)
        partial(slot_of(rr, ty(dy)), put)

    top, bottom = pl.ds(0, half_rows), pl.ds(half_rows, half_rows)

    def halves_out():
        for dy in others:
            i = at_of(1 - r, yat(dy))
            k = dy - 1
            send(pc_r.at[i, top], hx_r.at[k], hx_ss.at[k], hx_rs.at[k], x_dev)
            send(pc_r.at[i, bottom], hy_r.at[k], hy_ss.at[k], hy_rs.at[k], y_dev(dy))

    EC = 64

    def add_rows(i, base, terms):
        @pl.loop(0, half_rows // EC)
        def _(k):
            at = pl.ds(pl.multiple_of(base + k * EC, EC), EC)
            total = pc_r[i, at].astype(F32)
            for term in terms:
                total += term[pl.ds(pl.multiple_of(k * EC, EC), EC)].astype(F32)
            pc_r[i, at] = total.astype(BF16)

    def blocks_out():
        for dy in others:
            i = at_of(r, yat(dy))
            arrived(hx_r.at[dy - 1], hx_rs.at[dy - 1])
            add_rows(i, 0, [hx_r.at[dy - 1]])
            send(pc_r.at[i], py_r.at[dy - 1], py_ss.at[dy - 1], py_rs.at[dy - 1], y_dev(dy))
        i = at_of(1 - r, y)
        for dy in others:
            arrived(hy_r.at[dy - 1], hy_rs.at[dy - 1])
        add_rows(i, half_rows, [hy_r.at[dy - 1] for dy in others])
        send(pc_r.at[i], px_r, px_ss, px_rs, x_dev)

    def tokens_final():
        i = at_of(r, y)
        for dy in others:
            arrived(py_r.at[dy - 1], py_rs.at[dy - 1])
        arrived(px_r, px_rs)

        @pl.loop(0, R // EC)
        def _(k):
            at = rows(k * EC, EC)
            total = pc_r[i, at].astype(F32) + px_r[at].astype(F32)
            for dy in others:
                total += py_r[dy - 1, at].astype(F32)
            gt_out[at] = total.astype(BF16)

    def squares(value):
        return jnp.sum(value * value, axis=0, keepdims=True)

    def finish(w, buf, out, at):
        value = buf.astype(F32)
        turned = value.T
        if w == DOWN:
            out[at] = buf
            return squares(turned)
        if sliced:
            out[:, rows(at * H, H)] = turned.astype(BF16)
        else:
            out[at] = turned.astype(BF16)
        return squares(value)

    def finish_wide(w, row, out):
        arrived(xr.at[w], x_recv.at[w])
        tnorm[t, pl.ds(row, 1)] = finish(w, xs[w], out, r) + finish(w, xr[w], out, 1 - r)

    def finish_down():
        arrived(xr.at[DOWN], x_recv.at[DOWN])
        fnorm[f, pl.ds(r, 1)] = finish(DOWN, xs[DOWN], gd_out, r)
        fnorm[f, pl.ds(1 - r, 1)] = finish(DOWN, xr[DOWN], gd_out, 1 - r)

    def norms_out(table, me, count, ss, rsem, dev):
        for i in range(1, count):
            send(table.at[me], table.at[me], ss.at[i - 1], rsem.at[me], dev(i))

    def norms_in(table, me, count, rsem, out):
        for i in range(1, count):
            k = lax.rem(me + i, count)
            arrived(table.at[k], rsem.at[k])
        out[...] = jnp.sum(table[...], axis=0)

    order = []
    for g in range((groups + 1) // 2):
        order += [groups - 1 - g] + ([g] if g < groups - 1 - g else [])

    for load in loads[:3]:
        load.wait()
    tok_out(1, 0)
    weights_step(GATE, 0)
    weights_step(UP, 0)
    tok_out(0, 1)
    for h in (0, 1):
        send_piece(*tok_piece(mine, h), core_dev)
    for load in loads[3:]:
        load.wait()
    for g in order:
        send_piece(*cot_piece(mine, g, None), core_dev)
    tnorm[t] = jnp.zeros(tnorm.shape[1:], F32)
    fnorm[f] = jnp.zeros(fnorm.shape[1:], F32)
    if n > 2:
        weights_step(GATE, 1)
    tok_first()
    cot_out(order[0])
    tok_first_core()
    if n > 2:
        weights_step(UP, 1)
    tok_second()
    if groups > 1:
        cot_out(order[1])
    for s in range(2, n - 1):
        weights_step(GATE, s)
        weights_step(UP, s)
    weights_step(DOWN, 0)
    tok_diagonal()
    tok_from_core()
    steps = T // MB
    gate_up_most(0, steps // 2)

    def cot_next(k):
        cot_first(order[k])
        if k + 2 < groups:
            cot_out(order[k + 2])
        cot_first_core(order[k])

    cot_next(0)
    gate_up_most(steps // 2, steps)
    if groups > 1:
        cot_next(1)
    weights_step(GATE, n - 1)
    weights_step(UP, n - 1)
    cot_diagonal(order[0])
    gate_up_last()
    if groups > 2:
        cot_next(2)
    cot_from_core(order[0])
    grad_edge_group(DOWN, order[0])
    down_steps = list(range(1, n - 1))
    for s in down_steps[:1]:
        weights_step(DOWN, s)
    for k in range(1, groups):
        cot_diagonal(order[k])
        if k + 2 < groups:
            cot_next(k + 2)
        cot_from_core(order[k])
        grad_edge_group(DOWN, order[k])
        for s in down_steps[k:k + 1]:
            weights_step(DOWN, s)
    for s in down_steps[groups:]:
        weights_step(DOWN, s)
    if n > 2:
        grad_through(DOWN, n - 2, 2)
    weights_step(DOWN, n - 1)
    hidden_grads()
    grad_edge_all(GATE)
    if n > 2:
        grad_through(DOWN, 1, 1)
    pieces = ([(1 - r, dy) for dy in others] + [(r, dy) for dy in others] + [(1 - r, 0), (r, 0)])
    for rr, dy in pieces:
        partial_for_core(rr, dy)
    for rr, dy in pieces[:len(others)]:
        partial_own(rr, dy)
    halves_out()
    for rr, dy in pieces[len(others):]:
        partial_own(rr, dy)
    if n > 2:
        grad_through(GATE, n - 2, 2)
    grad_final(DOWN)
    grad_edge_all(UP)
    blocks_out()
    if n > 2:
        grad_through(GATE, 1, 1)
    finish_down()
    norms_out(fnorm, f, n, fn_ss, fn_rs, lambda i: (r, lax.rem(f + i, n), t))
    if n > 2:
        grad_through(UP, n - 2, 2)
    grad_final(GATE)
    if n > 2:
        grad_through(UP, 1, 1)
    tokens_final()
    finish_wide(GATE, 0, gg_out)
    norms_in(fnorm, f, n, fn_rs, fn_out)
    grad_final(UP)
    finish_wide(UP, 1, gu_out)
    norms_out(tnorm, t, tps, tn_ss, tn_rs, lambda i: (r, f, lax.rem(t + i, tps)))
    norms_in(tnorm, t, tps, tn_rs, tn_out)

    for copy in pending:
        copy.wait_send()
    for w in (DOWN, GATE, UP):
        weights_sent(w)
        grads_sent(w)
        remote(xs.at[w], xr.at[w], x_send.at[w], x_recv.at[w], x_dev).wait_send()


def local(tokens, cotangent, gate_weight, up_weight, down_weight):
    n, tps = lax.axis_size("fs"), lax.axis_size("tp")
    ny = tps // 2
    R, D = tokens.shape
    H = gate_weight.shape[1] // 2
    T, Dn = 2 * tps * R, D // n
    sliced = H % 128 == 0
    if not sliced:
        r = lax.axis_index("rep")
        gate_weight = lax.dynamic_slice_in_dim(gate_weight, r * H, H, 1)
        up_weight = lax.dynamic_slice_in_dim(up_weight, r * H, H, 1)
        down_weight = lax.dynamic_slice_in_dim(down_weight, r * H, H, 0)
    blocks = 2 * tps
    groups = min(n, 4)
    wide_shape = (Dn, 2 * H) if sliced else (2, Dn, H)
    more = max(ny - 1, 1)
    vmem = pltpu.VMEM
    dma = lambda *shape: pltpu.SemaphoreType.DMA(shape)
    shape = jax.ShapeDtypeStruct
    any_spec, vmem_spec = pl.BlockSpec(memory_space=pl.ANY), pl.BlockSpec(memory_space=vmem)
    flops = 2 * 8 * T * D * H
    gt, gg, gu, gd, tn, fn = pl.pallas_call(
        functools.partial(kernel, n, tps, sliced, groups),
        out_shape=(
            shape((R, D), BF16), shape(wide_shape, BF16), shape(wide_shape, BF16),
            shape((2, H, Dn), BF16), shape((8, Dn), F32), shape((8, H), F32)),
        in_specs=[any_spec] * 5,
        out_specs=(vmem_spec,) * 6,
        scratch_shapes=[
            vmem((T, D), BF16), vmem((T, D), BF16),
            vmem((D, H), BF16), vmem((D, H), BF16), vmem((H, D), BF16),
            vmem((T, H), F32), vmem((T, H), F32), vmem((T, H), F32),
            vmem((H, T), BF16), vmem((H, T), BF16), vmem((H, T), BF16),
            vmem((T, H), BF16), vmem((T, H), BF16), vmem((H, Dn), F32),
            vmem((3, n + 1, H, Dn), BF16), vmem((3, H, Dn), BF16), vmem((3, H, Dn), BF16),
            vmem((2 * ny, R, D), BF16), vmem((2 * ny, R, D), BF16),
            vmem((more, R // 2, D), BF16), vmem((more, R // 2, D), BF16),
            vmem((more, R, D), BF16), vmem((R, D), BF16),
            vmem((tps, 8, Dn), F32), vmem((n, 8, H), F32),
            dma(5), dma(12 * ny * (groups + 1)), dma(blocks, 2), dma(blocks, groups, 2),
            dma(3, 2, n), dma(3, n), dma(3, n), dma(3, n + 1), dma(3), dma(3),
            dma(2 * ny), dma(2 * ny), dma(more), dma(more), dma(more), dma(more),
            dma(more), dma(more), pltpu.SemaphoreType.DMA, pltpu.SemaphoreType.DMA,
            dma(tps), dma(tps), dma(n), dma(n),
        ],
        compiler_params=pltpu.CompilerParams(
            collective_id=0, has_side_effects=True, vmem_limit_bytes=67043328),
        cost_estimate=pl.CostEstimate(flops=flops, bytes_accessed=16 << 20, transcendentals=T * H),
    )(tokens, cotangent, gate_weight, up_weight, down_weight)
    def wide(part):
        if not sliced:
            part = jnp.concatenate([part[0], part[1]], axis=1)
        return part.astype(F32)
    return (
        gt,
        wide(gg),
        wide(gu),
        gd.reshape(2 * H, Dn).astype(F32),
        tn[0],
        tn[1],
        jnp.concatenate([fn[0], fn[1]]),
    )


def solution(mesh):
    placed = (
        P(("rep", "fs", "tp"), None),
        P(("rep", "fs", "tp"), None),
        P("fs", "tp"),
        P("fs", "tp"),
        P("tp", "fs"),
    )
    return jax.shard_map(
        local,
        mesh=mesh,
        in_specs=placed,
        out_specs=(
            P(("rep", "fs", "tp"), None),
            P("fs", "tp"),
            P("fs", "tp"),
            P("tp", "fs"),
            P("fs"),
            P("fs"),
            P("tp"),
        ),
        check_vma=False,
    )
```

time: 220 us -> 184 us (0.84)
  the two profiles are of different devices: /device:TPU:17 before, /device:TPU:0 now
where the time goes in v1:
time: 184 us; the launch traced here: 180 us
  Pallas kernels  171 us (93%)
  other arithmetic  5.65 us (3%)
  local copies, waits for them, and re-layouts  3.31 us (2%)
    pallas_call x1, Pallas kernels, local(): pl.pallas_call(functools.partial(kernel, n, tps, sliced, groups), out_sha...  171 us

profile of v1, /device:TPU:0, one launch (start us, length us, event | category | flops | bytes accessed | tf_op | source)
XLA Modules:
  0.0 180.5 jit_solution(7172715629815253483)
XLA Ops:
  0.6 170.9 %shard_map.108 = (bf16[256,2048]{1,0:T(8,128)(2,1)}, bf16[512,768]{1,0:T(8,128)(2,1)}, bf16[512,768]{1,0:T(8,128)(2,1)}, bf16[2,384,512]{2,1,0:T(8,128)(2,1)}, f32[8,512]{1,0:T(8,128)}, /*index=5*/f32[8,384]{1,0:T(8,128)}) custom-call(bf16[256,2048]{1,0:T(8,128)(2,1)} %tok_in.1, bf16[256,2048]{1,0:T(8,128)(2,1)} %cot_in.1, bf16[512,768]{1,0:T(8,128)(2,1)} %wg_in.1, ...), custom_call_target="tpu_custom_call" | custom-call | flops 25769803776 | bytes 16777216 | tf_op jit(solution)/shard_map/pallas_call | solution.py:551
  171.5 0.0 copy-start.2
  171.5 1.4 fusion
  172.9 0.8 slice_reduce_fusion.1
  173.7 0.6 pad_maximum_fusion
  174.3 2.4 %convert_element_type.12 = f32[512,768]{1,0:T(8,128)} convert(bf16[512,768]{1,0:T(8,128)(2,1)} %get-tuple-element.14) | non-fusion elementwise | flops 393216 | bytes 2359296 | tf_op jit(solution)/shard_map/convert_element_type | solution.py:582
  176.7 0.0 copy-done.2
  176.7 0.0 copy-start.1
  176.7 1.3 convert_element_type.13
  178.0 0.1 copy-done.1
  178.1 0.0 copy-start
  178.1 1.4 bitcast_convert_fusion
  179.5 0.0 copy-done
  179.5 1.0 copy.13
Async XLA Ops:
  171.5 5.2 %copy-start.2 = (bf16[512,768]{1,0:T(8,128)(2,1)S(1)}, bf16[512,768]{1,0:T(8,128)(2,1)}, u32[]{:S(2)}) copy-start(bf16[512,768]{1,0:T(8,128)(2,1)} %get-tuple-element.15) | copy-start | bytes 2359300
  176.7 1.4 copy-start.1
  178.1 1.4 copy-start

commit v2 on v1

--- a/solution.py
+++ b/solution.py
@@ -18,13 +18,13 @@
     )
 
 
-def kernel(n, tps, sliced, groups, tok_in, cot_in, wg_in, wu_in, wd_in,
+def kernel(n, tps, sliced, groups, cuts, tok_in, cot_in, wg_in, wu_in, wd_in,
            gt_out, gg_out, gu_out, gd_out, tn_out, fn_out,
            tok, cot, wg, wu, wd, act, coef, dh, hT, gT, uT, dg, du, own, rs, xs, xr,
-           pc_s, pc_r, hx_r, hy_r, py_r, px_r, tnorm, fnorm,
+           pc_s, pc_r, py_r, px_r, turned, tnorm, fnorm, t_sum, f_sum,
            load_sem, ag_send, tok_recv, cot_recv, z_send, z_recv, rs_send, rs_recv,
-           x_send, x_recv, pc_ss, pc_rs, hx_ss, hx_rs, hy_ss, hy_rs, py_ss, py_rs,
-           px_ss, px_rs, tn_ss, tn_rs, fn_ss, fn_rs):
+           x_send, x_recv, pc_ss, pc_rs, py_ss, py_rs, px_ss, px_rs,
+           tn_ss, tn_rs, fn_ss, fn_rs, out_sem):
     ny = tps // 2
     r, f, t = lax.axis_index("rep"), lax.axis_index("fs"), lax.axis_index("tp")
     y, c = lax.div(t, 2), lax.rem(t, 2)
@@ -76,8 +76,9 @@
         pl.semaphore_signal(barrier, inc=1, device_id=(r, f, lax.rem(t + i, tps)), device_id_type=MESH)
     for i in range(1, n):
         pl.semaphore_signal(barrier, inc=1, device_id=(r, lax.rem(f + i, n), t), device_id_type=MESH)
-    pl.semaphore_signal(barrier, inc=1, device_id=x_dev, device_id_type=MESH)
-    pl.semaphore_wait(barrier, tps - 1 + n - 1 + 1)
+    for i in range(tps):
+        pl.semaphore_signal(barrier, inc=1, device_id=(1 - r, f, lax.rem(t + i, tps)), device_id_type=MESH)
+    pl.semaphore_wait(barrier, tps - 1 + n - 1 + tps)
 
     sent = [0]
 
@@ -223,20 +224,28 @@
             coef[blk] = up * sig * (1.0 + gate * (1.0 - sig))
             hT[:, blk] = (a * up).astype(BF16).T
 
-    def hidden_grads():
+    def hidden_most():
         @pl.loop(0, T // MB)
         def _(i):
-            blk = rows(i * MB, MB)
-            dh[blk] = contract_last(cot[blk], wd[...])
+            blk, cols = rows(i * MB, MB), pl.ds(pl.multiple_of(most_at, Dn), most)
+            dh[blk] = contract_last(cot[blk, cols], wd[:, cols])
+
+    def hidden_last():
+        @pl.loop(0, T // MB)
+        def _(i):
+            blk, cols = rows(i * MB, MB), rows(last_at, Dn)
+            dh[blk] += contract_last(cot[blk, cols], wd[:, cols])
 
         @pl.loop(0, T // EB)
         def _(i):
             blk = rows(i * EB, EB)
+            slot, within = lax.div(i, R // EB), lax.rem(i, R // EB)
+            by_core = rows((lax.rem(slot, 2) * tps + lax.div(slot, 2)) * R + within * EB, EB)
             dhid = dh[blk]
             a = (dhid * coef[blk]).astype(BF16)
             b = (dhid * act[blk]).astype(BF16)
-            dg[blk] = a
-            du[blk] = b
+            dg[by_core] = a
+            du[by_core] = b
             gT[:, blk] = a.T
             uT[:, blk] = b.T
 
@@ -245,6 +254,19 @@
     def own_part(w, d):
         lhs, rhs = sources[w]
         own[...] = jnp.dot(lhs[...], rhs[:, rows(d * Dn, Dn)], preferred_element_type=F32)
+
+    strip = H // cuts
+
+    def strips(ref, w, k, q):
+        return ref.at[w, k, pl.ds(q * strip, strip)]
+
+    def grad_send(w, d, q, there, to):
+        remote(strips(rs, w, d, q), strips(rs, w, there, q), rs_send.at[w, d, q],
+               rs_recv.at[w, there, q], to).start()
+
+    def grad_add(w, k, q):
+        arrived(strips(rs, w, k, q), rs_recv.at[w, k, q])
+        return own[pl.ds(q * strip, strip)] + rs[w, k, pl.ds(q * strip, strip)].astype(F32)
 
     def grad_edge(w, d):
         @pl.when(jnp.where(f == 0, d > 0, jnp.logical_and(f == n - 1, d < n - 1)))
@@ -253,156 +275,201 @@
             rs[w, d] = own[...].astype(BF16)
             there = jnp.where(jnp.logical_and(f > 0, d == f - 1), n, d)
             to = (r, jnp.where(f == 0, 1, n - 2), t)
-            remote(rs.at[w, d], rs.at[w, there], rs_send.at[w, d], rs_recv.at[w, there], to).start()
+            for q in range(cuts):
+                grad_send(w, d, q, there, to)
 
     def grad_edge_group(w, g):
         per = n // groups
 
         @pl.loop(0, per)
         def _(i):
-            grad_edge(w, g * per + i)
-
-    def grad_edge_all(w):
-        @pl.loop(0, n - 1)
+            grad_edge(w, g * per + jnp.where(f == 0, per - 1 - i, i))
+
+    def grad_edges(w, first, last):
+        @pl.loop(first, last)
         def _(i):
             grad_edge(w, jnp.where(f == 0, n - 1 - i, i))
 
-    def grad_through(w, first, last):
-        @pl.loop(0, first - last + 1)
-        def _(i):
-            dist = first - i
-            for to, d, has in (
-                (right, f + dist, jnp.logical_and(f + dist < n, f > 0)),
-                (left, f - dist, jnp.logical_and(f - dist >= 0, f < n - 1)),
-            ):
-                @pl.when(has)
-                def _():
-                    own_part(w, d)
-                    arrived(rs.at[w, d], rs_recv.at[w, d])
-                    rs[w, d] = (own[...] + rs[w, d].astype(F32)).astype(BF16)
-                    there = d if to is right else jnp.where(d == f - 1, n, d)
-                    remote(rs.at[w, d], rs.at[w, there], rs_send.at[w, d], rs_recv.at[w, there], to).start()
+    def grad_through(w, dist, far):
+        onward = jnp.where((2 * f < n) == (not far), 1, -1)
+        d = f + dist * onward
+        here = jnp.logical_and(d >= 0, d < n)
+
+        @pl.when(jnp.logical_and(here, jnp.logical_and(f > 0, f < n - 1)))
+        def _():
+            own_part(w, d)
+            there = jnp.where(jnp.logical_and(onward < 0, d == f - 1), n, d)
+            for q in range(cuts):
+                rs[w, d, pl.ds(q * strip, strip)] = grad_add(w, d, q).astype(BF16)
+                grad_send(w, d, q, there, (r, f + onward, t))
+
+    def grad_through_far(w):
+        if n > 3:
+            @pl.loop(0, n - 3)
+            def _(i):
+                for far in (False, True):
+                    grad_through(w, n - 2 - i, far)
+
+    def grad_through_near(w, far):
+        if n > 2:
+            grad_through(w, 1, far)
 
     def grads_sent(w):
         @pl.loop(0, n)
         def _(d):
             @pl.when(d != f)
             def _():
-                remote(rs.at[w, d], rs.at[w, d], rs_send.at[w, d], rs_recv.at[w, d], right).wait_send()
+                for q in range(cuts):
+                    remote(strips(rs, w, d, q), strips(rs, w, d, q), rs_send.at[w, d, q],
+                           rs_recv.at[w, d, q], right).wait_send()
 
     def grad_final(w):
         own_part(w, f)
-
-        @pl.when(f > 0)
-        def _():
-            arrived(rs.at[w, f], rs_recv.at[w, f])
-            own[...] += rs[w, f].astype(F32)
-
-        @pl.when(f < n - 1)
-        def _():
-            arrived(rs.at[w, n], rs_recv.at[w, n])
-            own[...] += rs[w, n].astype(F32)
-
-        xs[w] = own[...].astype(BF16)
-        remote(xs.at[w], xr.at[w], x_send.at[w], x_recv.at[w], x_dev).start()
+        for q in range(cuts):
+            @pl.when(f > 0)
+            def _():
+                own[pl.ds(q * strip, strip)] = grad_add(w, f, q)
+
+            @pl.when(f < n - 1)
+            def _():
+                own[pl.ds(q * strip, strip)] = grad_add(w, n, q)
+
+            xs[w, pl.ds(q * strip, strip)] = own[pl.ds(q * strip, strip)].astype(BF16)
+            send(xs.at[w, pl.ds(q * strip, strip)], xr.at[w, pl.ds(q * strip, strip)],
+                 x_send.at[w, q], x_recv.at[w, q], x_dev)
+
+    def halves_arrived(w):
+        for q in range(cuts):
+            arrived(xr.at[w, pl.ds(q * strip, strip)], x_recv.at[w, q])
 
     KB = min(512, D)
-
-    def partial(slot, finish):
-        blk = rows(slot * R, R)
+    at_of = lambda rr, yy: rr * ny + yy
+
+    def product(core, first, count, put):
+        blk = pl.ds(pl.multiple_of((core * 2 * ny + first) * R, R), count * R)
 
         @pl.loop(0, D // KB)
         def _(k):
             cols = rows(k * KB, KB)
-            finish(cols, contract_last(dg[blk], wg[cols]) + contract_last(du[blk], wu[cols]))
-
-    at_of = lambda rr, yy: rr * ny + yy
-
-    def partial_for_core(rr, dy):
-        i = at_of(rr, yat(dy))
+            put(cols, contract_last(dg[blk], wg[cols]) + contract_last(du[blk], wu[cols]))
+
+    def block(ref, rr, dy):
+        return ref.at[rows(at_of(rr, yat(dy)) * R, R)]
+
+    def tokens_for_core(rr):
+        blk = rows(rr * ny * R, ny * R)
 
         def put(cols, value):
-            pc_s[i, :, cols] = value.astype(BF16)
-        partial(slot_of(rr, cored(ty(dy))), put)
-        send(pc_s.at[i], pc_r.at[i], pc_ss.at[i], pc_rs.at[i], core_dev)
-
-    def partial_own(rr, dy):
-        i = at_of(rr, yat(dy))
-        arrived(pc_r.at[i], pc_rs.at[i])
-
-        def put(cols, value):
-            pc_r[i, :, cols] = (value + pc_r[i, :, cols].astype(F32)).astype(BF16)
-        partial(slot_of(rr, ty(dy)), put)
-
-    top, bottom = pl.ds(0, half_rows), pl.ds(half_rows, half_rows)
-
-    def halves_out():
-        for dy in others:
-            i = at_of(1 - r, yat(dy))
-            k = dy - 1
-            send(pc_r.at[i, top], hx_r.at[k], hx_ss.at[k], hx_rs.at[k], x_dev)
-            send(pc_r.at[i, bottom], hy_r.at[k], hy_ss.at[k], hy_rs.at[k], y_dev(dy))
-
-    EC = 64
-
-    def add_rows(i, base, terms):
-        @pl.loop(0, half_rows // EC)
+            pc_s[blk, cols] = value.astype(BF16)
+        product(1 - c, rr * ny, ny, put)
+        for dy in list(others) + [0]:
+            i = at_of(rr, yat(dy))
+            send(block(pc_s, rr, dy), block(pc_r, rr, dy), pc_ss.at[i], pc_rs.at[i], core_dev)
+
+    def tokens_own(rr, dys):
+        for dy in dys:
+            arrived(block(pc_r, rr, dy), pc_rs.at[at_of(rr, yat(dy))])
+        groups_of = [(rr * ny, ny)] if len(dys) == ny else [(at_of(rr, yat(dy)), 1) for dy in dys]
+        for first, count in groups_of:
+            blk = pl.ds(pl.multiple_of(first * R, R), count * R)
+
+            def put(cols, value):
+                pc_r[blk, cols] = (value + pc_r[blk, cols].astype(F32)).astype(BF16)
+            product(c, first, count, put)
+
+    quarter = R // 4
+    spans = [(k * quarter, quarter) for k in range(4)]
+    EC = R // 8
+
+    def span_at(ref, span):
+        return ref.at[pl.ds(span[0], span[1])]
+
+    def add_span(rr, dy, span, refs):
+        start = at_of(rr, yat(dy)) * R + span[0]
+
+        @pl.loop(0, span[1] // EC)
         def _(k):
-            at = pl.ds(pl.multiple_of(base + k * EC, EC), EC)
-            total = pc_r[i, at].astype(F32)
-            for term in terms:
-                total += term[pl.ds(pl.multiple_of(k * EC, EC), EC)].astype(F32)
-            pc_r[i, at] = total.astype(BF16)
-
-    def blocks_out():
-        for dy in others:
-            i = at_of(r, yat(dy))
-            arrived(hx_r.at[dy - 1], hx_rs.at[dy - 1])
-            add_rows(i, 0, [hx_r.at[dy - 1]])
-            send(pc_r.at[i], py_r.at[dy - 1], py_ss.at[dy - 1], py_rs.at[dy - 1], y_dev(dy))
-        i = at_of(1 - r, y)
-        for dy in others:
-            arrived(hy_r.at[dy - 1], hy_rs.at[dy - 1])
-        add_rows(i, half_rows, [hy_r.at[dy - 1] for dy in others])
-        send(pc_r.at[i], px_r, px_ss, px_rs, x_dev)
+            here = rows(start + k * EC, EC)
+            total = pc_r[here].astype(F32)
+            for ref in refs:
+                total += ref[rows(span[0] + k * EC, EC)].astype(F32)
+            pc_r[here] = total.astype(BF16)
+
+    def to_y(rr, which, dy, span, k):
+        send(span_at(block(pc_r, rr, dy), span), span_at(py_r.at[which, dy - 1], span),
+             py_ss.at[which, dy - 1, k], py_rs.at[which, dy - 1, k], y_dev(dy))
+
+    def from_y(which, dy, span, k):
+        arrived(span_at(py_r.at[which, dy - 1], span), py_rs.at[which, dy - 1, k])
+
+    def to_x(k):
+        send(span_at(block(pc_r, 1 - r, 0), spans[k]), span_at(px_r, spans[k]), px_ss.at[k], px_rs.at[k], x_dev)
+
+    def y_out(rr, which):
+        for k, span in enumerate(spans):
+            for dy in others:
+                to_y(rr, which, dy, span, k)
+
+    def x_piece(k):
+        for dy in others:
+            from_y(0, dy, spans[k], k)
+        add_span(1 - r, 0, spans[k], [py_r.at[0, dy - 1] for dy in others])
+        to_x(k)
 
     def tokens_final():
-        i = at_of(r, y)
-        for dy in others:
-            arrived(py_r.at[dy - 1], py_rs.at[dy - 1])
-        arrived(px_r, px_rs)
-
-        @pl.loop(0, R // EC)
-        def _(k):
-            at = rows(k * EC, EC)
-            total = pc_r[i, at].astype(F32) + px_r[at].astype(F32)
+        for k, span in enumerate(spans):
+            arrived(span_at(px_r, span), px_rs.at[k])
             for dy in others:
-                total += py_r[dy - 1, at].astype(F32)
-            gt_out[at] = total.astype(BF16)
+                from_y(1, dy, span, k)
+        add_span(r, 0, (0, R), [px_r] + [py_r.at[1, dy - 1] for dy in others])
+        put_out(block(pc_r, r, 0), gt_out, 0)
 
     def squares(value):
         return jnp.sum(value * value, axis=0, keepdims=True)
 
-    def finish(w, buf, out, at):
-        value = buf.astype(F32)
-        turned = value.T
-        if w == DOWN:
-            out[at] = buf
-            return squares(turned)
-        if sliced:
-            out[:, rows(at * H, H)] = turned.astype(BF16)
-        else:
-            out[at] = turned.astype(BF16)
-        return squares(value)
-
-    def finish_wide(w, row, out):
-        arrived(xr.at[w], x_recv.at[w])
-        tnorm[t, pl.ds(row, 1)] = finish(w, xs[w], out, r) + finish(w, xr[w], out, 1 - r)
+    outs = []
+
+    def put_out(src, dst, k):
+        copy = pltpu.make_async_copy(src, dst, out_sem.at[k])
+        copy.start()
+        outs.append(copy)
+
+    def turn(w, k, buf, at, out):
+        turned[w - 1, k] = buf[w].astype(F32).T.astype(BF16)
+        dst = out.at[:, rows(at * H, H)] if sliced else out.at[at]
+        put_out(turned.at[w - 1, k], dst, 2 * w + k + 1)
+
+    def wide_mine(w, out):
+        tnorm[mine, pl.ds(w - 1, 1)] = squares(xs[w].astype(F32))
+        turn(w, 0, xs, r, out)
+
+    def wide_theirs(w, out):
+        halves_arrived(w)
+        turn(w, 1, xr, 1 - r, out)
+
+    def wide_norms_out():
+        for i in range(2):
+            for k in range(tps):
+                if i or k:
+                    to = (r if i == 0 else 1 - r, f, lax.rem(t + k, tps))
+                    at = i * tps + k
+                    send(tnorm.at[mine], tnorm.at[mine], tn_ss.at[at], tn_rs.at[mine], to)
+
+    def wide_norms_in():
+        for i in range(2):
+            for k in range(tps):
+                if i or k:
+                    slot = slot_of(r if i == 0 else 1 - r, lax.rem(t + k, tps))
+                    arrived(tnorm.at[slot], tn_rs.at[slot])
+        t_sum[...] = jnp.sum(tnorm[...], axis=0)
+        put_out(t_sum, tn_out, 7)
 
     def finish_down():
-        arrived(xr.at[DOWN], x_recv.at[DOWN])
-        fnorm[f, pl.ds(r, 1)] = finish(DOWN, xs[DOWN], gd_out, r)
-        fnorm[f, pl.ds(1 - r, 1)] = finish(DOWN, xr[DOWN], gd_out, 1 - r)
+        for k, (buf, at) in enumerate(((xs, r), (xr, 1 - r))):
+            if k:
+                halves_arrived(DOWN)
+            put_out(buf.at[DOWN], gd_out.at[at], k + 1)
+            fnorm[f, pl.ds(at, 1)] = squares(buf[DOWN].astype(F32).T)
 
     def norms_out(table, me, count, ss, rsem, dev):
         for i in range(1, count):
@@ -412,11 +479,10 @@
         for i in range(1, count):
             k = lax.rem(me + i, count)
             arrived(table.at[k], rsem.at[k])
-        out[...] = jnp.sum(table[...], axis=0)
-
-    order = []
-    for g in range((groups + 1) // 2):
-        order += [groups - 1 - g] + ([g] if g < groups - 1 - g else [])
+        f_sum[...] = jnp.sum(table[...], axis=0)
+        put_out(f_sum, out, 8)
+
+    order = [jnp.where(2 * f < n, groups - 1 - g, g) for g in range(groups)]
 
     for load in loads[:3]:
         load.wait()
@@ -430,7 +496,7 @@
         load.wait()
     for g in order:
         send_piece(*cot_piece(mine, g, None), core_dev)
-    tnorm[t] = jnp.zeros(tnorm.shape[1:], F32)
+    tnorm[mine] = jnp.zeros(tnorm.shape[1:], F32)
     fnorm[f] = jnp.zeros(fnorm.shape[1:], F32)
     if n > 2:
         weights_step(GATE, 1)
@@ -478,53 +544,74 @@
             cot_next(k + 2)
         cot_from_core(order[k])
         grad_edge_group(DOWN, order[k])
+        if n == 4 and k == groups - 2:
+            grad_through_far(DOWN)
         for s in down_steps[k:k + 1]:
             weights_step(DOWN, s)
     for s in down_steps[groups:]:
         weights_step(DOWN, s)
-    if n > 2:
-        grad_through(DOWN, n - 2, 2)
+    if n != 4:
+        grad_through_far(DOWN)
+    hidden_most()
     weights_step(DOWN, n - 1)
-    hidden_grads()
-    grad_edge_all(GATE)
-    if n > 2:
-        grad_through(DOWN, 1, 1)
-    pieces = ([(1 - r, dy) for dy in others] + [(r, dy) for dy in others] + [(1 - r, 0), (r, 0)])
-    for rr, dy in pieces:
-        partial_for_core(rr, dy)
-    for rr, dy in pieces[:len(others)]:
-        partial_own(rr, dy)
-    halves_out()
-    for rr, dy in pieces[len(others):]:
-        partial_own(rr, dy)
-    if n > 2:
-        grad_through(GATE, n - 2, 2)
+    hidden_last()
+    grad_edges(GATE, 0, 1)
+    grad_through_near(DOWN, False)
+    grad_through_near(DOWN, True)
+    tokens_for_core(1 - r)
+    grad_edges(GATE, 1, n - 1)
+    tokens_for_core(r)
+    tokens_own(1 - r, list(others))
+    y_out(1 - r, 0)
     grad_final(DOWN)
-    grad_edge_all(UP)
-    blocks_out()
-    if n > 2:
-        grad_through(GATE, 1, 1)
+    grad_through_far(GATE)
+    tokens_own(1 - r, [0])
+    tokens_own(r, list(range(ny)))
+    y_out(r, 1)
+    grad_edges(UP, 0, n - 1)
+    grad_through_near(GATE, False)
+    x_piece(0)
     finish_down()
     norms_out(fnorm, f, n, fn_ss, fn_rs, lambda i: (r, lax.rem(f + i, n), t))
-    if n > 2:
-        grad_through(UP, n - 2, 2)
+    grad_through_near(GATE, True)
+    x_piece(1)
+    x_piece(2)
     grad_final(GATE)
-    if n > 2:
-        grad_through(UP, 1, 1)
+    x_piece(3)
+    wide_mine(GATE, gg_out)
+    grad_through_far(UP)
+    grad_through_near(UP, False)
+    grad_through_near(UP, True)
+    wide_theirs(GATE, gg_out)
+    grad_final(UP)
+    wide_mine(UP, gu_out)
+    wide_norms_out()
     tokens_final()
-    finish_wide(GATE, 0, gg_out)
+    wide_theirs(UP, gu_out)
     norms_in(fnorm, f, n, fn_rs, fn_out)
-    grad_final(UP)
-    finish_wide(UP, 1, gu_out)
-    norms_out(tnorm, t, tps, tn_ss, tn_rs, lambda i: (r, f, lax.rem(t + i, tps)))
-    norms_in(tnorm, t, tps, tn_rs, tn_out)
-
+    wide_norms_in()
+
+    for copy in outs:
+        copy.wait()
     for copy in pending:
         copy.wait_send()
     for w in (DOWN, GATE, UP):
         weights_sent(w)
         grads_sent(w)
-        remote(xs.at[w], xr.at[w], x_send.at[w], x_recv.at[w], x_dev).wait_send()
+
+
+def widen(gt, gg, gu, gd, tn, fn, gt_out, gg_out, gu_out, gd_out, g_norm, u_norm, d_norm):
+    gt_out[...] = gt[...]
+    for src, dst in ((gg, gg_out), (gu, gu_out), (gd, gd_out)):
+        dst[...] = src[...].astype(F32)
+    g_norm[...] = tn[0:1]
+    u_norm[...] = tn[1:2]
+    if len(d_norm.shape) == 1:
+        size = fn.shape[1]
+        d_norm[0:size] = fn[0]
+        d_norm[size:] = fn[1]
+    else:
+        d_norm[...] = fn[0:2]
 
 
 def local(tokens, cotangent, gate_weight, up_weight, down_weight):
@@ -540,21 +627,21 @@
         up_weight = lax.dynamic_slice_in_dim(up_weight, r * H, H, 1)
         down_weight = lax.dynamic_slice_in_dim(down_weight, r * H, H, 0)
     blocks = 2 * tps
-    groups = min(n, 4)
+    groups, cuts = min(n, 4), 4
     wide_shape = (Dn, 2 * H) if sliced else (2, Dn, H)
     more = max(ny - 1, 1)
     vmem = pltpu.VMEM
     dma = lambda *shape: pltpu.SemaphoreType.DMA(shape)
     shape = jax.ShapeDtypeStruct
-    any_spec, vmem_spec = pl.BlockSpec(memory_space=pl.ANY), pl.BlockSpec(memory_space=vmem)
+    any_spec = pl.BlockSpec(memory_space=pl.ANY)
     flops = 2 * 8 * T * D * H
     gt, gg, gu, gd, tn, fn = pl.pallas_call(
-        functools.partial(kernel, n, tps, sliced, groups),
+        functools.partial(kernel, n, tps, sliced, groups, cuts),
         out_shape=(
             shape((R, D), BF16), shape(wide_shape, BF16), shape(wide_shape, BF16),
             shape((2, H, Dn), BF16), shape((8, Dn), F32), shape((8, H), F32)),
         in_specs=[any_spec] * 5,
-        out_specs=(vmem_spec,) * 6,
+        out_specs=(any_spec,) * 6,
         scratch_shapes=[
             vmem((T, D), BF16), vmem((T, D), BF16),
             vmem((D, H), BF16), vmem((D, H), BF16), vmem((H, D), BF16),
@@ -562,33 +649,34 @@
             vmem((H, T), BF16), vmem((H, T), BF16), vmem((H, T), BF16),
             vmem((T, H), BF16), vmem((T, H), BF16), vmem((H, Dn), F32),
             vmem((3, n + 1, H, Dn), BF16), vmem((3, H, Dn), BF16), vmem((3, H, Dn), BF16),
-            vmem((2 * ny, R, D), BF16), vmem((2 * ny, R, D), BF16),
-            vmem((more, R // 2, D), BF16), vmem((more, R // 2, D), BF16),
-            vmem((more, R, D), BF16), vmem((R, D), BF16),
-            vmem((tps, 8, Dn), F32), vmem((n, 8, H), F32),
+            vmem((2 * ny * R, D), BF16), vmem((2 * ny * R, D), BF16),
+            vmem((2, more, R, D), BF16), vmem((R, D), BF16),
+            vmem((2, 2, Dn, H), BF16), vmem((blocks, 8, Dn), F32), vmem((n, 8, H), F32), vmem((8, Dn), F32), vmem((8, H), F32),
             dma(5), dma(12 * ny * (groups + 1)), dma(blocks, 2), dma(blocks, groups, 2),
-            dma(3, 2, n), dma(3, n), dma(3, n), dma(3, n + 1), dma(3), dma(3),
-            dma(2 * ny), dma(2 * ny), dma(more), dma(more), dma(more), dma(more),
-            dma(more), dma(more), pltpu.SemaphoreType.DMA, pltpu.SemaphoreType.DMA,
-            dma(tps), dma(tps), dma(n), dma(n),
+            dma(3, 2, n), dma(3, n), dma(3, n, cuts), dma(3, n + 1, cuts), dma(3, cuts), dma(3, cuts),
+            dma(2 * ny), dma(2 * ny), dma(2, more, 4), dma(2, more, 4), dma(4), dma(4),
+            dma(blocks), dma(blocks), dma(n), dma(n), dma(9),
         ],
         compiler_params=pltpu.CompilerParams(
             collective_id=0, has_side_effects=True, vmem_limit_bytes=67043328),
         cost_estimate=pl.CostEstimate(flops=flops, bytes_accessed=16 << 20, transcendentals=T * H),
     )(tokens, cotangent, gate_weight, up_weight, down_weight)
-    def wide(part):
-        if not sliced:
-            part = jnp.concatenate([part[0], part[1]], axis=1)
-        return part.astype(F32)
-    return (
-        gt,
-        wide(gg),
-        wide(gu),
-        gd.reshape(2 * H, Dn).astype(F32),
-        tn[0],
-        tn[1],
-        jnp.concatenate([fn[0], fn[1]]),
-    )
+    if not sliced:
+        gg, gu = (jnp.concatenate([part[0], part[1]], axis=1) for part in (gg, gu))
+    steps = 2
+    pieces = [(R, D), (Dn, 2 * H), (Dn, 2 * H), (2 * H, Dn)]
+    tiles = [pl.BlockSpec((rows // steps, cols), lambda i: (i, 0)) for rows, cols in pieces]
+    whole = lambda *dims: pl.BlockSpec(dims, lambda i: (0,) * len(dims))
+    norms = [(1, Dn), (1, Dn), (2 * H,) if sliced else (2, H)]
+    outs = pl.pallas_call(
+        widen,
+        grid=(steps,),
+        out_shape=[shape(piece, F32 if i else BF16) for i, piece in enumerate(pieces)]
+        + [shape(norm, F32) for norm in norms],
+        in_specs=tiles + [whole(8, Dn), whole(8, H)],
+        out_specs=tiles + [whole(*norm) for norm in norms],
+    )(gt, gg, gu, gd.reshape(2 * H, Dn), tn, fn)
+    return tuple(outs[:4]) + tuple(out.reshape(-1) for out in outs[4:])
 
 
 def solution(mesh):

time: 184 us -> 159 us (0.86); the launches traced: 180 us -> 159 us
  Pallas kernels: 171 us -> 158 us
  other arithmetic: 5.65 us -> 0 us
  local copies, waits for them, and re-layouts: 3.31 us -> 0 us
    pallas_call x1 -> x2, Pallas kernels: 171 us -> 158 us  [the longest x1 154 us: local(): pl.pallas_call(functools.partial(kernel, n, tps, sliced, groups, cuts), o...]
    convert_element_type x3 -> x0, other arithmetic: 5.04 us -> none  [the longest x2 3.64 us: wide(): return part.astype(F32)]
    slice x2 -> x0, local copies, waits for them, and re-layouts: 2.19 us -> none  [the longest x1 1.39 us: local(): tn[1]]
where the time goes in v2:
time: 159 us
  Pallas kernels  158 us (99%)
    pallas_call x1, Pallas kernels, local(): pl.pallas_call(functools.partial(kernel, n, tps, sliced, groups, cuts), o...  154 us
    pallas_call x1, Pallas kernels, local(): pl.pallas_call(widen, grid=(steps,), out_shape=[shape(piece, F32 if i els...  4.08 us

profile of v2, /device:TPU:0, one launch (start us, length us, event | category | flops | bytes accessed | tf_op | source)
XLA Modules:
  0.0 159.0 jit_solution(5563839848573112244)
XLA Ops:
  0.6 154.2 %shard_map.108 = (bf16[256,2048]{1,0:T(8,128)(2,1)}, bf16[512,768]{1,0:T(8,128)(2,1)}, bf16[512,768]{1,0:T(8,128)(2,1)}, bf16[2,384,512]{2,1,0:T(8,128)(2,1)}, f32[8,512]{1,0:T(8,128)}, /*index=5*/f32[8,384]{1,0:T(8,128)}) custom-call(bf16[256,2048]{1,0:T(8,128)(2,1)} %tok_in.1, bf16[256,2048]{1,0:T(8,128)(2,1)} %cot_in.1, bf16[512,768]{1,0:T(8,128)(2,1)} %wg_in.1, ...), custom_call_target="tpu_custom_call" | custom-call | flops 25769803776 | bytes 16777216 | tf_op jit(solution)/shard_map/pallas_call | solution.py:638
  154.9 4.1 %shard_map.109 = (bf16[256,2048]{1,0:T(8,128)(2,1)}, f32[512,768]{1,0:T(8,128)}, f32[512,768]{1,0:T(8,128)}, f32[768,512]{1,0:T(8,128)}, f32[1,512]{1,0:T(1,128)}, /*index=5*/f32[1,512]{1,0:T(1,128)}, f32[768]{0:T(1024)}) custom-call(bf16[256,2048]{1,0:T(8,128)(2,1)} %get-tuple-element.20.gt, bf16[512,768]{1,0:T(8,128)(2,1)} %get-tuple-element.21.gg, ...), custom_call_target="tpu_custom_call" | custom-call | tf_op jit(solution)/shard_map/pallas_call | solution.py:671

commit v3 on v2

--- a/solution.py
+++ b/solution.py
@@ -50,12 +50,11 @@
     def rows(start, size):
         return pl.ds(pl.multiple_of(start, size), size)
 
-    pending = []
-
     def send(*args):
-        copy = remote(*args)
-        copy.start()
-        pending.append(copy)
+        remote(*args).start()
+
+    def all_sent(view, sem):
+        remote(view, view, sem, sem, core_dev).wait_send()
 
     half = (lambda ref: ref.at[:, rows(r * H, H)]) if sliced else (lambda ref: ref)
     half_d = (lambda ref: ref.at[rows(r * H, H)]) if sliced else (lambda ref: ref)
@@ -80,11 +79,11 @@
         pl.semaphore_signal(barrier, inc=1, device_id=(1 - r, f, lax.rem(t + i, tps)), device_id_type=MESH)
     pl.semaphore_wait(barrier, tps - 1 + n - 1 + tps)
 
-    sent = [0]
-
-    def send_piece(view, sem, dev):
-        send(view, view, ag_send.at[sent[0]], sem, dev)
-        sent[0] += 1
+    sent = [0, 0]
+
+    def send_piece(view, sem, dev, a=0):
+        send(view, view, ag_send.at[a], sem, dev)
+        sent[a] += view.shape[0] * view.shape[1]
 
     slot_of = lambda rr, tt: rr * tps + tt
 
@@ -93,7 +92,7 @@
 
     def cot_piece(slot, g, h):
         at = rows(slot * R, R) if h is None else rows(slot * R + h * half_rows, half_rows)
-        return cot.at[at, rows(g * chunk, chunk)], cot_recv.at[slot, g, h or 0]
+        return cot.at[at, rows(g * chunk, chunk)], cot_recv.at[slot, g]
 
     mine, beside = slot_of(r, t), slot_of(1 - r, t)
     along = lambda dy: slot_of(r, ty(-dy))
@@ -135,36 +134,35 @@
                 for h in (0, 1):
                     arrived(*tok_piece(slot_of(rr, cored(ty(dy))), h))
 
+    def cot_send(slot, g, h, dev):
+        send_piece(*cot_piece(slot, g, h), dev, 1)
+
     def cot_out(g):
-        send_piece(*cot_piece(mine, g, None), x_dev)
-        for dy in others:
-            send_piece(*cot_piece(mine, g, None), y_dev(dy))
+        cot_send(mine, g, None, x_dev)
+        for dy in others:
+            cot_send(mine, g, None, y_dev(dy))
 
     def cot_first(g):
         arrived(*cot_piece(beside, g, None))
         for dy in others:
-            send_piece(*cot_piece(beside, g, 1), y_dev(dy))
+            cot_send(beside, g, 1, y_dev(dy))
         for dy in others:
             arrived(*cot_piece(along(dy), g, None))
-            send_piece(*cot_piece(along(dy), g, 0), x_dev)
+            cot_send(along(dy), g, 0, x_dev)
 
     def cot_first_core(g):
         for slot in [beside] + [along(dy) for dy in others]:
-            send_piece(*cot_piece(slot, g, None), core_dev)
+            cot_send(slot, g, None, core_dev)
 
     def cot_diagonal(g):
         for dy in others:
-            for h in (0, 1):
-                arrived(*cot_piece(diagonal(dy), g, h))
-                send_piece(*cot_piece(diagonal(dy), g, h), core_dev)
+            arrived(*cot_piece(diagonal(dy), g, None))
+            cot_send(diagonal(dy), g, None, core_dev)
 
     def cot_from_core(g):
-        arrived(*cot_piece(slot_of(r, tcore), g, None))
-        arrived(*cot_piece(slot_of(1 - r, tcore), g, None))
-        for dy in others:
-            arrived(*cot_piece(slot_of(r, cored(ty(dy))), g, None))
-            for h in (0, 1):
-                arrived(*cot_piece(slot_of(1 - r, cored(ty(dy))), g, h))
+        for dy in range(ny):
+            for rr in (r, 1 - r):
+                arrived(*cot_piece(slot_of(rr, cored(ty(dy))), g, None))
 
     def weight(w, k):
         if w == DOWN:
@@ -217,12 +215,17 @@
         @pl.loop(0, T // EB)
         def _(i):
             blk = rows(i * EB, EB)
+            gate = act[blk]
+            hT[:, blk] = (gate * jax.nn.sigmoid(gate) * coef[blk]).astype(BF16).T
+
+    def slopes():
+        @pl.loop(0, T // EB)
+        def _(i):
+            blk = rows(i * EB, EB)
             gate, up = act[blk], coef[blk]
             sig = jax.nn.sigmoid(gate)
-            a = gate * sig
-            act[blk] = a
+            act[blk] = gate * sig
             coef[blk] = up * sig * (1.0 + gate * (1.0 - sig))
-            hT[:, blk] = (a * up).astype(BF16).T
 
     def hidden_most():
         @pl.loop(0, T // MB)
@@ -261,7 +264,7 @@
         return ref.at[w, k, pl.ds(q * strip, strip)]
 
     def grad_send(w, d, q, there, to):
-        remote(strips(rs, w, d, q), strips(rs, w, there, q), rs_send.at[w, d, q],
+        remote(strips(rs, w, d, q), strips(rs, w, there, q), rs_send.at[w],
                rs_recv.at[w, there, q], to).start()
 
     def grad_add(w, k, q):
@@ -315,13 +318,8 @@
             grad_through(w, 1, far)
 
     def grads_sent(w):
-        @pl.loop(0, n)
-        def _(d):
-            @pl.when(d != f)
-            def _():
-                for q in range(cuts):
-                    remote(strips(rs, w, d, q), strips(rs, w, d, q), rs_send.at[w, d, q],
-                           rs_recv.at[w, d, q], right).wait_send()
+        all_sent(rs.at[w, pl.ds(0, n - 1)], rs_send.at[w])
+        all_sent(xs.at[w], x_send.at[w])
 
     def grad_final(w):
         own_part(w, f)
@@ -336,11 +334,10 @@
 
             xs[w, pl.ds(q * strip, strip)] = own[pl.ds(q * strip, strip)].astype(BF16)
             send(xs.at[w, pl.ds(q * strip, strip)], xr.at[w, pl.ds(q * strip, strip)],
-                 x_send.at[w, q], x_recv.at[w, q], x_dev)
+                 x_send.at[w], x_recv.at[w], x_dev)
 
     def halves_arrived(w):
-        for q in range(cuts):
-            arrived(xr.at[w, pl.ds(q * strip, strip)], x_recv.at[w, q])
+        arrived(xr.at[w], x_recv.at[w])
 
     KB = min(512, D)
     at_of = lambda rr, yy: rr * ny + yy
@@ -364,7 +361,7 @@
         product(1 - c, rr * ny, ny, put)
         for dy in list(others) + [0]:
             i = at_of(rr, yat(dy))
-            send(block(pc_s, rr, dy), block(pc_r, rr, dy), pc_ss.at[i], pc_rs.at[i], core_dev)
+            send(block(pc_s, rr, dy), block(pc_r, rr, dy), pc_ss, pc_rs.at[i], core_dev)
 
     def tokens_own(rr, dys):
         for dy in dys:
@@ -397,13 +394,13 @@
 
     def to_y(rr, which, dy, span, k):
         send(span_at(block(pc_r, rr, dy), span), span_at(py_r.at[which, dy - 1], span),
-             py_ss.at[which, dy - 1, k], py_rs.at[which, dy - 1, k], y_dev(dy))
+             py_ss.at[which], py_rs.at[which, dy - 1, k], y_dev(dy))
 
     def from_y(which, dy, span, k):
         arrived(span_at(py_r.at[which, dy - 1], span), py_rs.at[which, dy - 1, k])
 
     def to_x(k):
-        send(span_at(block(pc_r, 1 - r, 0), spans[k]), span_at(px_r, spans[k]), px_ss.at[k], px_rs.at[k], x_dev)
+        send(span_at(block(pc_r, 1 - r, 0), spans[k]), span_at(px_r, spans[k]), px_ss, px_rs.at[k], x_dev)
 
     def y_out(rr, which):
         for k, span in enumerate(spans):
@@ -452,15 +449,10 @@
             for k in range(tps):
                 if i or k:
                     to = (r if i == 0 else 1 - r, f, lax.rem(t + k, tps))
-                    at = i * tps + k
-                    send(tnorm.at[mine], tnorm.at[mine], tn_ss.at[at], tn_rs.at[mine], to)
+                    send(tnorm.at[mine], tnorm.at[mine], tn_ss, tn_rs, to)
 
     def wide_norms_in():
-        for i in range(2):
-            for k in range(tps):
-                if i or k:
-                    slot = slot_of(r if i == 0 else 1 - r, lax.rem(t + k, tps))
-                    arrived(tnorm.at[slot], tn_rs.at[slot])
+        arrived(tnorm.at[pl.ds(0, 2 * tps - 1)], tn_rs)
         t_sum[...] = jnp.sum(tnorm[...], axis=0)
         put_out(t_sum, tn_out, 7)
 
@@ -471,16 +463,14 @@
             put_out(buf.at[DOWN], gd_out.at[at], k + 1)
             fnorm[f, pl.ds(at, 1)] = squares(buf[DOWN].astype(F32).T)
 
-    def norms_out(table, me, count, ss, rsem, dev):
-        for i in range(1, count):
-            send(table.at[me], table.at[me], ss.at[i - 1], rsem.at[me], dev(i))
-
-    def norms_in(table, me, count, rsem, out):
-        for i in range(1, count):
-            k = lax.rem(me + i, count)
-            arrived(table.at[k], rsem.at[k])
-        f_sum[...] = jnp.sum(table[...], axis=0)
-        put_out(f_sum, out, 8)
+    def norms_out():
+        for i in range(1, n):
+            send(fnorm.at[f], fnorm.at[f], fn_ss, fn_rs, (r, lax.rem(f + i, n), t))
+
+    def norms_in():
+        arrived(fnorm.at[pl.ds(0, n - 1)], fn_rs)
+        f_sum[...] = jnp.sum(fnorm[...], axis=0)
+        put_out(f_sum, fn_out, 8)
 
     order = [jnp.where(2 * f < n, groups - 1 - g, g) for g in range(groups)]
 
@@ -495,7 +485,7 @@
     for load in loads[3:]:
         load.wait()
     for g in order:
-        send_piece(*cot_piece(mine, g, None), core_dev)
+        cot_send(mine, g, None, core_dev)
     tnorm[mine] = jnp.zeros(tnorm.shape[1:], F32)
     fnorm[f] = jnp.zeros(fnorm.shape[1:], F32)
     if n > 2:
@@ -535,6 +525,7 @@
         cot_next(2)
     cot_from_core(order[0])
     grad_edge_group(DOWN, order[0])
+    slopes()
     down_steps = list(range(1, n - 1))
     for s in down_steps[:1]:
         weights_step(DOWN, s)
@@ -572,7 +563,7 @@
     grad_through_near(GATE, False)
     x_piece(0)
     finish_down()
-    norms_out(fnorm, f, n, fn_ss, fn_rs, lambda i: (r, lax.rem(f + i, n), t))
+    norms_out()
     grad_through_near(GATE, True)
     x_piece(1)
     x_piece(2)
@@ -588,16 +579,23 @@
     wide_norms_out()
     tokens_final()
     wide_theirs(UP, gu_out)
-    norms_in(fnorm, f, n, fn_rs, fn_out)
+    norms_in()
     wide_norms_in()
 
     for copy in outs:
         copy.wait()
-    for copy in pending:
-        copy.wait_send()
+    for a, buf in enumerate((tok, cot)):
+        all_sent(buf.at[pl.ds(0, sent[a] // D)], ag_send.at[a])
     for w in (DOWN, GATE, UP):
         weights_sent(w)
         grads_sent(w)
+    all_sent(pc_s, pc_ss)
+    if ny > 1:
+        for which in (0, 1):
+            all_sent(py_r.at[which], py_ss.at[which])
+    all_sent(px_r, px_ss)
+    all_sent(tnorm.at[pl.ds(0, 2 * tps - 1)], tn_ss)
+    all_sent(fnorm.at[pl.ds(0, n - 1)], fn_ss)
 
 
 def widen(gt, gg, gu, gd, tn, fn, gt_out, gg_out, gu_out, gd_out, g_norm, u_norm, d_norm):
@@ -631,7 +629,8 @@
     wide_shape = (Dn, 2 * H) if sliced else (2, Dn, H)
     more = max(ny - 1, 1)
     vmem = pltpu.VMEM
-    dma = lambda *shape: pltpu.SemaphoreType.DMA(shape)
+    one = pltpu.SemaphoreType.DMA
+    dma = lambda *shape: one(shape)
     shape = jax.ShapeDtypeStruct
     any_spec = pl.BlockSpec(memory_space=pl.ANY)
     flops = 2 * 8 * T * D * H
@@ -652,10 +651,10 @@
             vmem((2 * ny * R, D), BF16), vmem((2 * ny * R, D), BF16),
             vmem((2, more, R, D), BF16), vmem((R, D), BF16),
             vmem((2, 2, Dn, H), BF16), vmem((blocks, 8, Dn), F32), vmem((n, 8, H), F32), vmem((8, Dn), F32), vmem((8, H), F32),
-            dma(5), dma(12 * ny * (groups + 1)), dma(blocks, 2), dma(blocks, groups, 2),
-            dma(3, 2, n), dma(3, n), dma(3, n, cuts), dma(3, n + 1, cuts), dma(3, cuts), dma(3, cuts),
-            dma(2 * ny), dma(2 * ny), dma(2, more, 4), dma(2, more, 4), dma(4), dma(4),
-            dma(blocks), dma(blocks), dma(n), dma(n), dma(9),
+            dma(5), dma(2), dma(blocks, 2), dma(blocks, groups),
+            dma(3, 2, n - 1), dma(3, n), dma(3), dma(3, n + 1, cuts), dma(3), dma(3),
+            one, dma(2 * ny), dma(2), dma(2, more, 4), one, dma(4),
+            one, one, one, one, dma(9),
         ],
         compiler_params=pltpu.CompilerParams(
             collective_id=0, has_side_effects=True, vmem_limit_bytes=67043328),

time: 159 us -> 157 us (0.987)
  Pallas kernels: 158 us -> 156 us
    pallas_call x1, Pallas kernels: 154 us -> 152 us  [local(): pl.pallas_call(functools.partial(kernel, n, tps, sliced, groups, cuts), o...]
where the time goes in v3:
time: 157 us; the launch traced here: 156 us
  Pallas kernels  156 us (99%)
    pallas_call x1, Pallas kernels, local(): pl.pallas_call(functools.partial(kernel, n, tps, sliced, groups, cuts), o...  152 us
    pallas_call x1, Pallas kernels, local(): pl.pallas_call(widen, grid=(steps,), out_shape=[shape(piece, F32 if i els...  4.08 us

profile of v3, /device:TPU:0, one launch (start us, length us, event | category | flops | bytes accessed | tf_op | source)
XLA Modules:
  0.0 156.5 jit_solution(435549312211858741)
XLA Ops:
  0.6 151.7 %shard_map.108 = (bf16[256,2048]{1,0:T(8,128)(2,1)}, bf16[512,768]{1,0:T(8,128)(2,1)}, bf16[512,768]{1,0:T(8,128)(2,1)}, bf16[2,384,512]{2,1,0:T(8,128)(2,1)}, f32[8,512]{1,0:T(8,128)}, /*index=5*/f32[8,384]{1,0:T(8,128)}) custom-call(bf16[256,2048]{1,0:T(8,128)(2,1)} %tok_in.1, bf16[256,2048]{1,0:T(8,128)(2,1)} %cot_in.1, bf16[512,768]{1,0:T(8,128)(2,1)} %wg_in.1, ...), custom_call_target="tpu_custom_call" | custom-call | flops 25769803776 | bytes 16777216 | tf_op jit(solution)/shard_map/pallas_call | solution.py:637
  152.3 4.1 %shard_map.109 = (bf16[256,2048]{1,0:T(8,128)(2,1)}, f32[512,768]{1,0:T(8,128)}, f32[512,768]{1,0:T(8,128)}, f32[768,512]{1,0:T(8,128)}, f32[1,512]{1,0:T(1,128)}, /*index=5*/f32[1,512]{1,0:T(1,128)}, f32[768]{0:T(1024)}) custom-call(bf16[256,2048]{1,0:T(8,128)(2,1)} %get-tuple-element.20.gt, bf16[512,768]{1,0:T(8,128)(2,1)} %get-tuple-element.21.gg, ...), custom_call_target="tpu_custom_call" | custom-call | tf_op jit(solution)/shard_map/pallas_call | solution.py:670

commit v4 on v3

--- a/solution.py
+++ b/solution.py
@@ -560,23 +560,23 @@
     tokens_own(r, list(range(ny)))
     y_out(r, 1)
     grad_edges(UP, 0, n - 1)
+    grad_through_near(GATE, True)
     grad_through_near(GATE, False)
     x_piece(0)
     finish_down()
     norms_out()
-    grad_through_near(GATE, True)
     x_piece(1)
     x_piece(2)
     grad_final(GATE)
     x_piece(3)
     wide_mine(GATE, gg_out)
     grad_through_far(UP)
+    grad_through_near(UP, True)
     grad_through_near(UP, False)
-    grad_through_near(UP, True)
-    wide_theirs(GATE, gg_out)
     grad_final(UP)
     wide_mine(UP, gu_out)
     wide_norms_out()
+    wide_theirs(GATE, gg_out)
     tokens_final()
     wide_theirs(UP, gu_out)
     norms_in()

time: 157 us -> 157 us (level)
  no operation moved by 1% of the time
where the time goes in v4:
time: 157 us; the launch traced here: 156 us
  Pallas kernels  156 us (99%)
    pallas_call x1, Pallas kernels, local(): pl.pallas_call(functools.partial(kernel, n, tps, sliced, groups, cuts), o...  152 us
    pallas_call x1, Pallas kernels, local(): pl.pallas_call(widen, grid=(steps,), out_shape=[shape(piece, F32 if i els...  4.08 us

profile of v4, /device:TPU:0, one launch (start us, length us, event | category | flops | bytes accessed | tf_op | source)
XLA Modules:
  0.0 156.5 jit_solution(14731242379383673674)
XLA Ops:
  0.6 151.7 %shard_map.108 = (bf16[256,2048]{1,0:T(8,128)(2,1)}, bf16[512,768]{1,0:T(8,128)(2,1)}, bf16[512,768]{1,0:T(8,128)(2,1)}, bf16[2,384,512]{2,1,0:T(8,128)(2,1)}, f32[8,512]{1,0:T(8,128)}, /*index=5*/f32[8,384]{1,0:T(8,128)}) custom-call(bf16[256,2048]{1,0:T(8,128)(2,1)} %tok_in.1, bf16[256,2048]{1,0:T(8,128)(2,1)} %cot_in.1, bf16[512,768]{1,0:T(8,128)(2,1)} %wg_in.1, ...), custom_call_target="tpu_custom_call" | custom-call | flops 25769803776 | bytes 16777216 | tf_op jit(solution)/shard_map/pallas_call | solution.py:637
  152.3 4.1 %shard_map.109 = (bf16[256,2048]{1,0:T(8,128)(2,1)}, f32[512,768]{1,0:T(8,128)}, f32[512,768]{1,0:T(8,128)}, f32[768,512]{1,0:T(8,128)}, f32[1,512]{1,0:T(1,128)}, /*index=5*/f32[1,512]{1,0:T(1,128)}, f32[768]{0:T(1024)}) custom-call(bf16[256,2048]{1,0:T(8,128)(2,1)} %get-tuple-element.20.gt, bf16[512,768]{1,0:T(8,128)(2,1)} %get-tuple-element.21.gg, ...), custom_call_target="tpu_custom_call" | custom-call | tf_op jit(solution)/shard_map/pallas_call | solution.py:670
